TPU v7x, 512 devices: a whole 4x4x16 slice. The times are simulated.
512 devices in a mesh: sp: 128 (over z, x, core), tp: 4 (over y).
Axes of the slice: x: 4, y: 4, z: 16, core: 2. Of those that a mesh axis runs over, the one named last changes fastest.
Arguments:
- tokens: bfloat16 [32768, 2048], P('sp'), may hold values from -6 to 6
- documents: int32 [32768], P('sp'), may hold values from 0 to 63, never falling along the last dimension, each value on 1 to 1024 neighbouring positions
- norm_gain: float32 [1, 2048], replicated, may hold values from 0.1 to 1.9
- w_query: bfloat16 [1, 2048, 2048], P(None, 'sp', 'tp'), may hold values from -0.125 to 0.125
- w_key: bfloat16 [1, 2048, 2048], P(None, 'sp', 'tp'), may hold values from -0.125 to 0.125
- w_value: bfloat16 [1, 2048, 2048], P(None, 'sp', 'tp'), may hold values from -0.125 to 0.125
- w_out: bfloat16 [1, 2048, 2048], P(None, None, 'sp'), may hold values from -0.59765625 to 0.59765625
- rel_bias: float32 [1, 32, 257], P(None, 'tp'), may hold values from -8 to 240
Outputs:
- mixed: bfloat16 [32768, 2048], P('sp')
Inputs may be any that keep to these rules, and one draw needn't show every extreme that they name: `documents`: document numbers never fall along the sequence; a document has 1 to 1024 positions.
All inputs are finite; a program needn't handle non-finite values.
Results may differ from a plain program's by a relative error of at most 0.007.
Values may be sent and summed in bfloat16 or wider, within the bound.
No kernel may reach another device: no remote copies, remote signals or barrier semaphores. Data moves between devices by JAX's collectives and lax.ppermute only.
A program may use at most 128 MiB of HBM per device.

v0:
```python
import jax
import jax.numpy as jnp
from jax import lax
from jax.experimental import pallas as pl
from jax.experimental.pallas import tpu as pltpu
from jax.sharding import Mesh
from jax.sharding import PartitionSpec as P

HEAD_DIM = 64
SEG = 64
LEFT = 4
REL_CLIP = 128
EPS = 1e-06
REACH = LEFT * SEG
Q_BLOCK = 2 * SEG
K_BLOCK = Q_BLOCK + REACH
SP = ("zh", "zl", "x", "c")
Z = ("zh", "zl")
NEG = -1e30


def to_all(x, axis):
    length = lax.axis_size(axis)
    return lax.all_to_all(jnp.broadcast_to(x[None], (length, *x.shape)), axis, 0, 0, tiled=True)


def prep_kernel(ids, w_q, w_k, w_v, w_o, tokens, gain, docs, heads, rest, block):
    n = heads.shape[0]
    own = w_o[:, pl.ds(pl.multiple_of(ids[3] * n * HEAD_DIM, n * HEAD_DIM), n * HEAD_DIM)]
    for i in range(n):
        cols = slice(i * HEAD_DIM, (i + 1) * HEAD_DIM)
        heads[i] = jnp.concatenate([w_q[:, cols], w_k[:, cols], w_v[:, cols]], axis=1)
        rest[i] = own[:, cols]
    rows = tokens.shape[0]
    wide = tokens[...].astype(jnp.float32)
    scale = lax.rsqrt(jnp.mean(wide * wide, axis=1, keepdims=True) + EPS)
    block[:rows, :] = (wide * scale * gain[...]).astype(jnp.bfloat16)
    extra = block.shape[0] - rows
    block[rows:, :rows] = jnp.broadcast_to(docs[...].astype(jnp.float32), (extra, rows)).astype(jnp.bfloat16)
    block[rows:, rows:] = jnp.zeros((extra, block.shape[1] - rows), jnp.bfloat16)


def sum_kernel(partial, tokens, out):
    total = tokens[...].astype(jnp.float32)
    for i in range(partial.shape[0]):
        total = total + partial[i].astype(jnp.float32)
    total = total.astype(jnp.bfloat16)
    for i in range(out.shape[0]):
        out[i] = total


def qkv_kernel(ids, b0, s0, b1, s1, b2, s2, b3, s3, w_in, qkv, docs, tail):
    rows = qkv.shape[0] // 8
    core, x = ids[0], ids[1]
    for back, pair in enumerate(((b0, s0), (b1, s1), (b2, s2), (b3, s3))):
        for c, part in zip((core, 1 - core), pair):
            at = ((x + 4 - back) & 3) * 2 + c
            total = jnp.dot(part[:rows, :], w_in[...], preferred_element_type=jnp.float32)
            qkv[pl.ds(pl.multiple_of(at * rows, rows), rows), :] = total.astype(jnp.bfloat16)
            docs[pl.ds(at, 1), :] = part[rows : rows + 16, :rows].astype(jnp.float32)[0:1]
    tail[:rows, :] = qkv[7 * rows :, :]
    tail[rows:, :] = jnp.broadcast_to(docs[7:8, :], (16, rows)).astype(jnp.bfloat16)


def attend(blocks, ids, qkv, halo, docs, line, out):
    rows = docs.shape[1]
    flat = jnp.broadcast_to(line[...], (Q_BLOCK, line.shape[1]))
    bias = pltpu.roll(flat, 0, 1, stride=1, stride_axis=0)[:, :K_BLOCK]
    q_seg = lax.broadcasted_iota(jnp.int32, (Q_BLOCK, K_BLOCK), 0) // SEG
    k_seg = lax.broadcasted_iota(jnp.int32, (Q_BLOCK, K_BLOCK), 1) // SEG
    bias = jnp.where((k_seg >= q_seg) & (k_seg <= q_seg + LEFT), bias, NEG)
    if halo is not None:
        prior = jnp.where(ids[2] > 0, halo[rows : rows + 16, :].astype(jnp.float32)[0:1], -1.0)

    def doc_part(b):
        if b < 0:
            return prior[:, rows + b * Q_BLOCK : rows + (b + 1) * Q_BLOCK]
        at = b * Q_BLOCK % rows
        return docs[b * Q_BLOCK // rows : b * Q_BLOCK // rows + 1, at : at + Q_BLOCK]

    def row_part(b, cols):
        if b < 0:
            return halo[rows + b * Q_BLOCK : rows + (b + 1) * Q_BLOCK, cols]
        return qkv[b * Q_BLOCK : (b + 1) * Q_BLOCK, cols]

    def key_rows(b, cols):
        if b >= 2:
            return qkv[(b - 2) * Q_BLOCK : (b + 1) * Q_BLOCK, cols]
        return jnp.concatenate([row_part(i, cols) for i in range(b - 2, b + 1)], axis=0)

    for b in blocks:
        across = jnp.broadcast_to(doc_part(b), (Q_BLOCK, Q_BLOCK)).T
        same = jnp.concatenate([across == doc_part(i) for i in range(b - 2, b + 1)], axis=1)
        scores = lax.dot_general(
            qkv[b * Q_BLOCK : (b + 1) * Q_BLOCK, :HEAD_DIM],
            key_rows(b, slice(HEAD_DIM, 2 * HEAD_DIM)),
            (((1,), (1,)), ((), ())),
            preferred_element_type=jnp.float32,
        )
        scores = jnp.where(same, scores * HEAD_DIM ** (-0.5) + bias, NEG)
        peak = jnp.max(scores, axis=1, keepdims=True)
        raised = jnp.exp(scores - peak)
        total = jnp.sum(raised, axis=1, keepdims=True)
        mixed = jnp.dot(
            raised.astype(jnp.bfloat16),
            key_rows(b, slice(2 * HEAD_DIM, 3 * HEAD_DIM)),
            preferred_element_type=jnp.float32,
        )
        lane = b % 2 * HEAD_DIM
        out[b // 2, :, lane : lane + HEAD_DIM] = (mixed / total).astype(jnp.bfloat16)


def later_kernel(qkv, docs, line, out):
    out[0] = jnp.zeros(out.shape[1:], out.dtype)
    attend(range(2, qkv.shape[0] // Q_BLOCK), None, qkv, None, docs, line, out)


def early_kernel(ids, qkv, halo, docs, line, later, out):
    out[1:] = later[1:]
    attend(range(2), ids, qkv, halo, docs, line, out)


def order_kernel(ids, own, below, above, low, high, w_all, rows_out):
    lanes = own.shape[1]
    for ahead, part, first in ((0, own, 0), (3, below, 0), (1, above, 0), (2, low, 0), (2, high, low.shape[0])):
        for i in range(part.shape[0]):
            z = (first + i) * 4 + ((ids[2] + ahead) & 3)
            w_all[pl.ds(pl.multiple_of(z * lanes, lanes), lanes), :] = part[i]
            rows_out[pl.ds(pl.multiple_of(z * 16, 16), 16), :] = jnp.concatenate(
                [part[i, 16 * j : 16 * j + 16, 3 * HEAD_DIM :] for j in range(8)], axis=1
            )


def project_kernel(ids, att, w_mine, w_other, out, lhs, rhs):
    half = att.shape[1]
    for i in range(att.shape[0]):
        lhs[:half, i * HEAD_DIM : (i + 1) * HEAD_DIM] = att[i, :, :HEAD_DIM]
        lhs[half:, i * HEAD_DIM : (i + 1) * HEAD_DIM] = att[i, :, HEAD_DIM:]
    core = ids[0]
    for c, w in ((core, w_mine), (1 - core, w_other)):
        for z in range(16):
            for x in range(4):
                to = pl.multiple_of(z * 128 + x * 32 + c * 16, 16)
                rhs[pl.ds(to, 16), :] = w[x, z * 16 : z * 16 + 16, :]
    out[...] = lax.dot_general(
        lhs[...], rhs[...], (((1,), (1,)), ((), ())), preferred_element_type=jnp.float32
    ).astype(jnp.bfloat16)


def in_vmem(kernel, outs, scratch=(), grant=16, flops=2 * 10**10):
    one = not isinstance(outs, (list, tuple))
    shapes = [outs] if one else list(outs)
    specs = [pl.BlockSpec(memory_space=pltpu.VMEM) for _ in shapes]

    def call(*args):
        return pl.pallas_call(
            kernel,
            out_shape=shapes[0] if one else shapes,
            in_specs=[pl.BlockSpec(memory_space=pltpu.SMEM if a.ndim == 1 else pltpu.VMEM) for a in args],
            out_specs=specs[0] if one else specs,
            scratch_shapes=list(scratch),
            compiler_params=pltpu.CompilerParams(vmem_limit_bytes=grant and grant * 2**20),
            cost_estimate=pl.CostEstimate(flops=flops, bytes_accessed=4 * 2**20, transcendentals=0),
        )(*args)

    return call


def bias_line(table):
    far = table[:, 2 * REL_CLIP :]
    near = table[:, 1:][:, ::-1]
    heads = table.shape[0]
    return jnp.concatenate(
        [
            jnp.broadcast_to(far, (heads, REACH - REL_CLIP)),
            near,
            table[:, :1],
            jnp.broadcast_to(far, (heads, Q_BLOCK - 1)),
        ],
        axis=1,
    )


def body(tokens, documents, norm_gain, w_query, w_key, w_value, w_out, rel_bias):
    rows, width = tokens.shape
    local = w_query.shape[2]
    core = lax.axis_index("c")
    x = lax.axis_index("x")
    z = lax.axis_index(Z)
    tp = lax.axis_index("tp")
    n_tp = lax.axis_size("tp")
    plane = ("x", "c")
    group = lax.axis_size(plane)
    bf = jnp.bfloat16

    piece = w_query.shape[1]
    ids = jnp.stack([core, x, z, tp])
    sources = (w_query[0], w_key[0], w_value[0], w_out[0].T, tokens, norm_gain, documents[None, :])
    packed, rest, block = in_vmem(
        prep_kernel,
        [
            jax.ShapeDtypeStruct((group, piece, 3 * HEAD_DIM), bf),
            jax.ShapeDtypeStruct((group, piece, HEAD_DIM), bf),
            jax.ShapeDtypeStruct((rows + 16, width), bf),
        ],
        grant=None,
        flops=10**9,
    )(ids, *sources)

    share = rows // n_tp
    at = lax.dynamic_slice_in_dim(tokens, tp * share, share, 0)
    line = bias_line(lax.dynamic_slice_in_dim(rel_bias[0], x * 2 + core, 1, 0))
    swap = [(0, 1), (1, 0)]
    parts = [block, lax.ppermute(block, "c", swap)]
    mine = lax.all_to_all(packed, plane, 0, 0, tiled=True)
    mine = jnp.concatenate([mine, rest], axis=2).reshape(group * piece, 4 * HEAD_DIM)
    for back in (1, 2, 3):
        got = lax.ppermute(block, "x", [(i, (i + back) % 4) for i in range(4)])
        parts += [got, lax.ppermute(got, "c", swap)]
    over_far = to_all(mine, "zh")
    over_far, line, at = lax.optimization_barrier((over_far, line, at))
    near = []
    two = over_far.shape[0] // 2
    for by, part in ((1, over_far), (-1, over_far), (2, over_far[:two]), (-2, over_far[two:])):
        near.append(lax.ppermute(part, Z, [(n, (n + by) % 16) for n in range(16)]))
    w_in, rows_out = in_vmem(
        order_kernel,
        [
            jax.ShapeDtypeStruct((width, 4 * HEAD_DIM), bf),
            jax.ShapeDtypeStruct((16 * piece, local), bf),
        ],
        flops=10**9,
    )(ids, over_far, *near)
    w_mine = to_all(rows_out, "x")
    w_other = lax.ppermute(w_mine, "c", swap)
    qkv, docs, tail = in_vmem(
        qkv_kernel,
        [
            jax.ShapeDtypeStruct((group * rows, 4 * HEAD_DIM), bf),
            jax.ShapeDtypeStruct((group, rows), jnp.float32),
            jax.ShapeDtypeStruct((rows + 16, 4 * HEAD_DIM), bf),
        ],
        grant=None,
    )(ids, *parts, w_in)
    halo = lax.ppermute(tail, Z, [(i, i + 1) for i in range(15)])
    att_shape = jax.ShapeDtypeStruct((group, rows // 2, 2 * HEAD_DIM), bf)
    att = in_vmem(later_kernel, att_shape)(qkv, docs, line)
    att = in_vmem(early_kernel, att_shape, flops=10**9)(ids, qkv, halo, docs, line, att)
    att = lax.all_to_all(att, plane, 0, 0, tiled=True)
    partial = in_vmem(
        project_kernel,
        jax.ShapeDtypeStruct((rows, width), bf),
        [pltpu.VMEM((rows, local), bf), pltpu.VMEM((width, local), bf)],
    )(ids, att, w_mine, w_other)
    partial = lax.all_to_all(partial.reshape(n_tp, share, width), "tp", 0, 0, tiled=True)
    mixed = in_vmem(sum_kernel, jax.ShapeDtypeStruct((n_tp, share, width), bf), flops=10**8)(partial, at)
    return lax.all_to_all(mixed, "tp", 0, 0, tiled=True).reshape(rows, width)


def solution(mesh):
    split = Mesh(mesh.devices.reshape(4, 4, 4, 2, mesh.shape["tp"]), (*SP, "tp"))
    placed = (
        P(SP, None),
        P(SP),
        P(),
        P(None, SP, "tp"),
        P(None, SP, "tp"),
        P(None, SP, "tp"),
        P(None, None, SP),
        P(None, "tp", None),
    )

    def step(*args):
        return body(*args)

    step = jax.shard_map(step, mesh=split, in_specs=placed, out_specs=P(SP, None), check_vma=False)
    return step
```

profile of v0, /device:TPU:96, one launch (start us, length us, event | category | flops | bytes accessed | tf_op | source)
XLA Modules:
  0.0 180.6 jit_solution(17448839336208083253)
XLA Ops:
  0.6 2.8 %shard_map.82 = (bf16[8,16,192]{2,1,0:T(8,128)(2,1)}, bf16[8,16,64]{2,1,0:T(8,128)(2,1)}, bf16[272,2048]{1,0:T(8,128)(2,1)}) custom-call(s32[4]{0:T(128)} %pad_add_fusion.ids, bf16[16,512]{1,0:T(8,128)(2,1)} %bitcast.25, bf16[16,512]{1,0:T(8,128)(2,1)} %bitcast.26, bf16[16,512]{1,0:T(8,128)(2,1)} %bitcast.27, bf16[16,2048]{1,0:T(8,128)(2,1)} %bitcast.24, ...), custom_call_target="tpu_custom_call" | custom-call | flops 1000000000 | bytes 4194304 | tf_op jit(solution)/shard_map/pallas_call | solution.py:156
  3.4 10.1 %all_to_all.30 = bf16[8,16,192]{2,1,0:T(8,128)(2,1)S(1)} all-to-all(bf16[8,16,192]{2,1,0:T(8,128)(2,1)} %get-tuple-element.17), channel_id=1, replica_groups=mesh['zh'=4,'zl'=4,'x'=4,'c'=2,'tp'=4] {'x','c'}, dimensions={0} | all-to-all | bytes 98304 | tf_op jit(solution)/shard_map/all_to_all | solution.py:215
  15.0 12.4 %all-to-all-start.1 = ((bf16[4,128,256]{2,1,0:T(8,128)(2,1)}), bf16[4,128,256]{2,1,0:T(8,128)(2,1)S(1)}, u32[]{:S(2)}, u32[]{:S(2)}) async-start(bf16[4,128,256]{2,1,0:T(8,128)(2,1)} %broadcast_in_dim.30), calls=%async_computation.1 | async-start | bytes 524288 | tf_op jit(solution)/shard_map/all_to_all | solution.py:24
  27.4 2.5 %collective-permute-start.1 = (bf16[272,2048]{1,0:T(8,128)(2,1)S(1)}, bf16[272,2048]{1,0:T(8,128)(2,1)}, u32[]{:S(2)}, u32[]{:S(2)}) collective-permute-start(bf16[272,2048]{1,0:T(8,128)(2,1)S(1)} %copy-done.6), channel_id=1, source_target_pairs={{0,8},{8,16},{16,24},{24,0},{1,9},{9,17},{17,25},{25,1},{2,10},{10... | collective-permute-start | bytes 3342344 | tf_op jit(solution)/shard_map/ppermute | solution.py:218
  29.9 4.0 %collective-permute-start.3 = (bf16[272,2048]{1,0:T(8,128)(2,1)S(1)}, bf16[272,2048]{1,0:T(8,128)(2,1)}, u32[]{:S(2)}, u32[]{:S(2)}) collective-permute-start(bf16[272,2048]{1,0:T(8,128)(2,1)S(1)} %copy-done.6), channel_id=1, source_target_pairs={{0,16},{8,24},{16,0},{24,8},{1,17},{9,25},{17,1},{25,9},{2,18},{10... | collective-permute-start | bytes 3342344 | tf_op jit(solution)/shard_map/ppermute | solution.py:218
  33.9 2.9 %collective-permute-start.5 = (bf16[272,2048]{1,0:T(8,128)(2,1)S(1)}, bf16[272,2048]{1,0:T(8,128)(2,1)}, u32[]{:S(2)}, u32[]{:S(2)}) collective-permute-start(bf16[272,2048]{1,0:T(8,128)(2,1)S(1)} %copy-done.6), channel_id=1, source_target_pairs={{0,24},{8,0},{16,8},{24,16},{1,25},{9,1},{17,9},{25,17},{2,26},{10... | collective-permute-start | bytes 3342344 | tf_op jit(solution)/shard_map/ppermute | solution.py:218
  40.6 4.6 %all-to-all-done.1.own = bf16[4,128,256]{2,1,0:T(8,128)(2,1)S(1)} async-done(((bf16[4,128,256]{2,1,0:T(8,128)(2,1)}), bf16[4,128,256]{2,1,0:T(8,128)(2,1)S(1)}, u32[]{:S(2)}, u32[]{:S(2)}) %all-to-all-start.1) | async-done | bytes 262176 | tf_op jit(solution)/shard_map/all_to_all | solution.py:24
  45.2 5.5 %collective-permute-start.9 = (bf16[2,128,256]{2,1,0:T(8,128)(2,1)S(1)}, bf16[2,128,256]{2,1,0:T(8,128)(2,1)S(1)}, u32[]{:S(2)}, u32[]{:S(2)}) collective-permute-start(bf16[2,128,256]{2,1,0:T(8,128)(2,1)S(1)} %get-tuple-element.28), channel_id=1, source_target_pairs={{0,64},{32,96},{64,128},{96,160},{128,192},{160,224},{192,256},{22... | collective-permute-start | bytes 393224 | tf_op jit(solution)/shard_map/ppermute | solution.py:225
  50.7 1.9 %collective-permute-start.7 = (bf16[4,128,256]{2,1,0:T(8,128)(2,1)S(1)}, bf16[4,128,256]{2,1,0:T(8,128)(2,1)S(1)}, u32[]{:S(2)}, u32[]{:S(2)}) collective-permute-start(bf16[4,128,256]{2,1,0:T(8,128)(2,1)S(1)} %all-to-all-done.1.own), channel_id=1, source_target_pairs={{0,32},{32,64},{64,96},{96,128},{128,160},{160,192},{192,224},{224... | collective-permute-start | bytes 786440 | tf_op jit(solution)/shard_map/ppermute | solution.py:225
  52.7 4.1 %collective-permute-done.9.low = bf16[2,128,256]{2,1,0:T(8,128)(2,1)S(1)} collective-permute-done((bf16[2,128,256]{2,1,0:T(8,128)(2,1)S(1)}, bf16[2,128,256]{2,1,0:T(8,128)(2,1)S(1)}, u32[]{:S(2)}, u32[]{:S(2)}) %collective-permute-start.9) | collective-permute-done | bytes 131104 | tf_op jit(solution)/shard_map/ppermute | solution.py:225
  56.8 5.0 %collective-permute-start.10 = (bf16[2,128,256]{2,1,0:T(8,128)(2,1)S(1)}, bf16[2,128,256]{2,1,0:T(8,128)(2,1)S(1)}, u32[]{:S(2)}, u32[]{:S(2)}) collective-permute-start(bf16[2,128,256]{2,1,0:T(8,128)(2,1)S(1)} %get-tuple-element.27), channel_id=1, source_target_pairs={{0,448},{32,480},{64,0},{96,32},{128,64},{160,96},{192,128},{224,1... | collective-permute-start | bytes 393224 | tf_op jit(solution)/shard_map/ppermute | solution.py:225
  61.9 3.9 %collective-permute-done.10.high = bf16[2,128,256]{2,1,0:T(8,128)(2,1)S(1)} collective-permute-done((bf16[2,128,256]{2,1,0:T(8,128)(2,1)S(1)}, bf16[2,128,256]{2,1,0:T(8,128)(2,1)S(1)}, u32[]{:S(2)}, u32[]{:S(2)}) %collective-permute-start.10) | collective-permute-done | bytes 131104 | tf_op jit(solution)/shard_map/ppermute | solution.py:225
  65.8 6.2 %collective-permute-start.8 = (bf16[4,128,256]{2,1,0:T(8,128)(2,1)S(1)}, bf16[4,128,256]{2,1,0:T(8,128)(2,1)S(1)}, u32[]{:S(2)}, u32[]{:S(2)}) collective-permute-start(bf16[4,128,256]{2,1,0:T(8,128)(2,1)S(1)} %all-to-all-done.1.own), channel_id=1, source_target_pairs={{0,480},{32,0},{64,32},{96,64},{128,96},{160,128},{192,160},{224,1... | collective-permute-start | bytes 786440 | tf_op jit(solution)/shard_map/ppermute | solution.py:225
  71.9 1.9 %collective-permute-start = (bf16[272,2048]{1,0:T(8,128)(2,1)S(1)}, bf16[272,2048]{1,0:T(8,128)(2,1)S(1)}, u32[]{:S(2)}, u32[]{:S(2)}) collective-permute-start(bf16[272,2048]{1,0:T(8,128)(2,1)S(1)} %copy-done.6), channel_id=1, source_target_pairs={{0,4},{4,0},{1,5},{5,1},{2,6},{6,2},{3,7},{7,3},{8,12},{12,8},{9,1... | collective-permute-start | bytes 3342344 | tf_op jit(solution)/shard_map/ppermute | solution.py:214
  73.9 6.5 %collective-permute-done.1.b1 = bf16[272,2048]{1,0:T(8,128)(2,1)} collective-permute-done((bf16[272,2048]{1,0:T(8,128)(2,1)S(1)}, bf16[272,2048]{1,0:T(8,128)(2,1)}, u32[]{:S(2)}, u32[]{:S(2)}) %collective-permute-start.1) | collective-permute-done | bytes 1114144 | tf_op jit(solution)/shard_map/ppermute | solution.py:218
  82.3 2.4 %collective-permute-start.4 = (bf16[272,2048]{1,0:T(8,128)(2,1)}, bf16[272,2048]{1,0:T(8,128)(2,1)S(1)}, u32[]{:S(2)}, u32[]{:S(2)}) collective-permute-start(bf16[272,2048]{1,0:T(8,128)(2,1)} %collective-permute-done.3.b2), channel_id=1, source_target_pairs={{0,4},{4,0},{1,5},{5,1},{2,6},{6,2},{3,7},{7,3},{8,12},{12,8},{9,1... | collective-permute-start | bytes 3342344 | tf_op jit(solution)/shard_map/ppermute | solution.py:219
  84.7 1.9 %collective-permute-start.6 = (bf16[272,2048]{1,0:T(8,128)(2,1)}, bf16[272,2048]{1,0:T(8,128)(2,1)S(1)}, u32[]{:S(2)}, u32[]{:S(2)}) collective-permute-start(bf16[272,2048]{1,0:T(8,128)(2,1)} %collective-permute-done.5.b3), channel_id=1, source_target_pairs={{0,4},{4,0},{1,5},{5,1},{2,6},{6,2},{3,7},{7,3},{8,12},{12,8},{9,1... | collective-permute-start | bytes 3342344 | tf_op jit(solution)/shard_map/ppermute | solution.py:219
  87.5 18.5 %all_to_all.31.w_mine = bf16[4,256,512]{2,1,0:T(8,128)(2,1)S(1)} all-to-all(bf16[4,256,512]{2,1,0:T(8,128)(2,1)S(1)} %broadcast_in_dim.34), channel_id=1, replica_groups=mesh['zh'=4,'zl'=4,'x'=4,'c'=2,'tp'=4] {'x'}, dimensions={0} | all-to-all | bytes 2097152 | tf_op jit(solution)/shard_map/all_to_all | solution.py:24
  112.1 7.2 %shard_map.84 = (bf16[2048,256]{1,0:T(8,128)(2,1)}, f32[8,256]{1,0:T(8,128)}, bf16[272,256]{1,0:T(8,128)(2,1)}) custom-call(s32[4]{0:T(128)} %pad_add_fusion.ids, bf16[272,2048]{1,0:T(8,128)(2,1)} %get-tuple-element.16.b0, bf16[272,2048]{1,0:T(8,128)(2,1)} %copy-done.7, bf16[272,2048]{1,0:T(8,128)(2,1)} %collective-permute-done.1.b1, ...), custom_call_target="tpu_custom_call" | custom-call | flops 20000000000 | bytes 4194304 | tf_op jit(solution)/shard_map/pallas_call | solution.py:156
  119.3 6.2 %collective-permute-start.11 = (bf16[272,256]{1,0:T(8,128)(2,1)}, bf16[272,256]{1,0:T(8,128)(2,1)S(1)}, u32[]{:S(2)}, u32[]{:S(2)}) collective-permute-start(bf16[272,256]{1,0:T(8,128)(2,1)} %get-tuple-element.22), channel_id=1, source_target_pairs={{0,32},{32,64},{64,96},{96,128},{128,160},{160,192},{192,224},{224... | collective-permute-start | bytes 417800 | tf_op jit(solution)/shard_map/ppermute | solution.py:245
  127.4 4.2 %shard_map.85.later = bf16[8,128,128]{2,1,0:T(8,128)(2,1)S(1)} custom-call(bf16[2048,256]{1,0:T(8,128)(2,1)S(1)} %copy-done.3, f32[8,256]{1,0:T(8,128)S(1)} %copy-done.5, f32[1,512]{1,0:T(1,128)S(1)} %maximum_maximum_fusion.line), custom_call_target="tpu_custom_call" | custom-call | flops 20000000000 | bytes 4194304 | tf_op jit(solution)/shard_map/pallas_call | solution.py:156
  133.1 9.9 %all_to_all.32.att = bf16[8,128,128]{2,1,0:T(8,128)(2,1)S(1)} all-to-all(bf16[8,128,128]{2,1,0:T(8,128)(2,1)S(1)} %shard_map.86), channel_id=1, replica_groups=mesh['zh'=4,'zl'=4,'x'=4,'c'=2,'tp'=4] {'x','c'}, dimensions={0} | all-to-all | bytes 524288 | tf_op jit(solution)/shard_map/all_to_all | solution.py:249
  144.4 19.0 %all_to_all.33.partial = bf16[4,64,2048]{2,1,0:T(8,128)(2,1)S(1)} all-to-all(bf16[4,64,2048]{2,1,0:T(8,128)(2,1)S(1)} %bitcast.19), channel_id=1, replica_groups=mesh['zh'=4,'zl'=4,'x'=4,'c'=2,'tp'=4] {'tp'}, dimensions={0} | all-to-all | bytes 2097152 | tf_op jit(solution)/shard_map/all_to_all | solution.py:255
  163.6 16.0 %all_to_all.34 = bf16[4,64,2048]{2,1,0:T(8,128)(2,1)S(1)} all-to-all(bf16[4,64,2048]{2,1,0:T(8,128)(2,1)S(1)} %shard_map.88), channel_id=1, replica_groups=mesh['zh'=4,'zl'=4,'x'=4,'c'=2,'tp'=4] {'tp'}, dimensions={0} | all-to-all | bytes 2097152 | tf_op jit(solution)/shard_map/all_to_all | solution.py:257
  (54 shorter events, 20.7 us)
Async XLA Ops:
  0.0 36.8 %copy-start = (f32[1,8,257]{2,1,0:T(8,128)S(1)}, f32[1,8,257]{2,1,0:T(8,128)}, u32[]{:S(2)}) copy-start(f32[1,8,257]{2,1,0:T(8,128)} %param.15) | copy-start | bytes 24676
  3.4 24.0 %copy-start.6 = (bf16[272,2048]{1,0:T(8,128)(2,1)S(1)}, bf16[272,2048]{1,0:T(8,128)(2,1)}, u32[]{:S(2)}) copy-start(bf16[272,2048]{1,0:T(8,128)(2,1)} %get-tuple-element.16.b0) | copy-start | bytes 3342340
  3.4 83.3 %copy-start.1 = (s32[4]{0:T(128)S(1)}, s32[4]{0:T(128)}, u32[]{:S(2)}) copy-start(s32[4]{0:T(128)} %pad_add_fusion.ids) | copy-start | bytes 52
  15.0 30.2 %all-to-all-start.1 = ((bf16[4,128,256]{2,1,0:T(8,128)(2,1)}), bf16[4,128,256]{2,1,0:T(8,128)(2,1)S(1)}, u32[]{:S(2)}, u32[]{:S(2)}) async-start(bf16[4,128,256]{2,1,0:T(8,128)(2,1)} %broadcast_in_dim.30), calls=%async_computation.1 | async-start | bytes 524288 | tf_op jit(solution)/shard_map/all_to_all | solution.py:24
  27.4 53.0 %collective-permute-start.1 = (bf16[272,2048]{1,0:T(8,128)(2,1)S(1)}, bf16[272,2048]{1,0:T(8,128)(2,1)}, u32[]{:S(2)}, u32[]{:S(2)}) collective-permute-start(bf16[272,2048]{1,0:T(8,128)(2,1)S(1)} %copy-done.6), channel_id=1, source_target_pairs={{0,8},{8,16},{16,24},{24,0},{1,9},{9,17},{17,25},{25,1},{2,10},{10... | collective-permute-start | bytes 3342344 | tf_op jit(solution)/shard_map/ppermute | solution.py:218
  29.9 52.4 %collective-permute-start.3 = (bf16[272,2048]{1,0:T(8,128)(2,1)S(1)}, bf16[272,2048]{1,0:T(8,128)(2,1)}, u32[]{:S(2)}, u32[]{:S(2)}) collective-permute-start(bf16[272,2048]{1,0:T(8,128)(2,1)S(1)} %copy-done.6), channel_id=1, source_target_pairs={{0,16},{8,24},{16,0},{24,8},{1,17},{9,25},{17,1},{25,9},{2,18},{10... | collective-permute-start | bytes 3342344 | tf_op jit(solution)/shard_map/ppermute | solution.py:218
  33.9 50.9 %collective-permute-start.5 = (bf16[272,2048]{1,0:T(8,128)(2,1)S(1)}, bf16[272,2048]{1,0:T(8,128)(2,1)}, u32[]{:S(2)}, u32[]{:S(2)}) collective-permute-start(bf16[272,2048]{1,0:T(8,128)(2,1)S(1)} %copy-done.6), channel_id=1, source_target_pairs={{0,24},{8,0},{16,8},{24,16},{1,25},{9,1},{17,9},{25,17},{2,26},{10... | collective-permute-start | bytes 3342344 | tf_op jit(solution)/shard_map/ppermute | solution.py:218
  45.2 11.6 %collective-permute-start.9 = (bf16[2,128,256]{2,1,0:T(8,128)(2,1)S(1)}, bf16[2,128,256]{2,1,0:T(8,128)(2,1)S(1)}, u32[]{:S(2)}, u32[]{:S(2)}) collective-permute-start(bf16[2,128,256]{2,1,0:T(8,128)(2,1)S(1)} %get-tuple-element.28), channel_id=1, source_target_pairs={{0,64},{32,96},{64,128},{96,160},{128,192},{160,224},{192,256},{22... | collective-permute-start | bytes 393224 | tf_op jit(solution)/shard_map/ppermute | solution.py:225
  50.7 21.2 %collective-permute-start.7 = (bf16[4,128,256]{2,1,0:T(8,128)(2,1)S(1)}, bf16[4,128,256]{2,1,0:T(8,128)(2,1)S(1)}, u32[]{:S(2)}, u32[]{:S(2)}) collective-permute-start(bf16[4,128,256]{2,1,0:T(8,128)(2,1)S(1)} %all-to-all-done.1.own), channel_id=1, source_target_pairs={{0,32},{32,64},{64,96},{96,128},{128,160},{160,192},{192,224},{224... | collective-permute-start | bytes 786440 | tf_op jit(solution)/shard_map/ppermute | solution.py:225
  56.8 9.0 %collective-permute-start.10 = (bf16[2,128,256]{2,1,0:T(8,128)(2,1)S(1)}, bf16[2,128,256]{2,1,0:T(8,128)(2,1)S(1)}, u32[]{:S(2)}, u32[]{:S(2)}) collective-permute-start(bf16[2,128,256]{2,1,0:T(8,128)(2,1)S(1)} %get-tuple-element.27), channel_id=1, source_target_pairs={{0,448},{32,480},{64,0},{96,32},{128,64},{160,96},{192,128},{224,1... | collective-permute-start | bytes 393224 | tf_op jit(solution)/shard_map/ppermute | solution.py:225
  65.8 20.9 %collective-permute-start.8 = (bf16[4,128,256]{2,1,0:T(8,128)(2,1)S(1)}, bf16[4,128,256]{2,1,0:T(8,128)(2,1)S(1)}, u32[]{:S(2)}, u32[]{:S(2)}) collective-permute-start(bf16[4,128,256]{2,1,0:T(8,128)(2,1)S(1)} %all-to-all-done.1.own), channel_id=1, source_target_pairs={{0,480},{32,0},{64,32},{96,64},{128,96},{160,128},{192,160},{224,1... | collective-permute-start | bytes 786440 | tf_op jit(solution)/shard_map/ppermute | solution.py:225
  71.9 35.9 %collective-permute-start = (bf16[272,2048]{1,0:T(8,128)(2,1)S(1)}, bf16[272,2048]{1,0:T(8,128)(2,1)S(1)}, u32[]{:S(2)}, u32[]{:S(2)}) collective-permute-start(bf16[272,2048]{1,0:T(8,128)(2,1)S(1)} %copy-done.6), channel_id=1, source_target_pairs={{0,4},{4,0},{1,5},{5,1},{2,6},{6,2},{3,7},{7,3},{8,12},{12,8},{9,1... | collective-permute-start | bytes 3342344 | tf_op jit(solution)/shard_map/ppermute | solution.py:214
  80.4 28.5 %collective-permute-start.2 = (bf16[272,2048]{1,0:T(8,128)(2,1)}, bf16[272,2048]{1,0:T(8,128)(2,1)S(1)}, u32[]{:S(2)}, u32[]{:S(2)}) collective-permute-start(bf16[272,2048]{1,0:T(8,128)(2,1)} %collective-permute-done.1.b1), channel_id=1, source_target_pairs={{0,4},{4,0},{1,5},{5,1},{2,6},{6,2},{3,7},{7,3},{8,12},{12,8},{9,1... | collective-permute-start | bytes 3342344 | tf_op jit(solution)/shard_map/ppermute | solution.py:219
  82.3 27.6 %collective-permute-start.4 = (bf16[272,2048]{1,0:T(8,128)(2,1)}, bf16[272,2048]{1,0:T(8,128)(2,1)S(1)}, u32[]{:S(2)}, u32[]{:S(2)}) collective-permute-start(bf16[272,2048]{1,0:T(8,128)(2,1)} %collective-permute-done.3.b2), channel_id=1, source_target_pairs={{0,4},{4,0},{1,5},{5,1},{2,6},{6,2},{3,7},{7,3},{8,12},{12,8},{9,1... | collective-permute-start | bytes 3342344 | tf_op jit(solution)/shard_map/ppermute | solution.py:219
  84.7 26.2 %collective-permute-start.6 = (bf16[272,2048]{1,0:T(8,128)(2,1)}, bf16[272,2048]{1,0:T(8,128)(2,1)S(1)}, u32[]{:S(2)}, u32[]{:S(2)}) collective-permute-start(bf16[272,2048]{1,0:T(8,128)(2,1)} %collective-permute-done.5.b3), channel_id=1, source_target_pairs={{0,4},{4,0},{1,5},{5,1},{2,6},{6,2},{3,7},{7,3},{8,12},{12,8},{9,1... | collective-permute-start | bytes 3342344 | tf_op jit(solution)/shard_map/ppermute | solution.py:219
  87.4 18.6 %copy-start.4 = (bf16[2048,256]{1,0:T(8,128)(2,1)}, bf16[2048,256]{1,0:T(8,128)(2,1)S(1)}, u32[]{:S(2)}) copy-start(bf16[2048,256]{1,0:T(8,128)(2,1)S(1)} %get-tuple-element.20.w_in) | copy-start | bytes 3145732
  106.0 37.0 %collective-permute-start.12 = (bf16[4,256,512]{2,1,0:T(8,128)(2,1)S(1)}, bf16[4,256,512]{2,1,0:T(8,128)(2,1)S(1)}, u32[]{:S(2)}, u32[]{:S(2)}) collective-permute-start(bf16[4,256,512]{2,1,0:T(8,128)(2,1)S(1)} %all_to_all.31.w_mine), channel_id=1, source_target_pairs={{0,4},{4,0},{1,5},{5,1},{2,6},{6,2},{3,7},{7,3},{8,12},{12,8},{9,1... | collective-permute-start | bytes 3145736 | tf_op jit(solution)/shard_map/ppermute | solution.py:235
  107.9 1.0 copy-start.7
  108.9 1.0 copy-start.8
  109.9 1.0 copy-start.9
  111.0 1.1 copy-start.10
  119.3 12.4 %collective-permute-start.11 = (bf16[272,256]{1,0:T(8,128)(2,1)}, bf16[272,256]{1,0:T(8,128)(2,1)S(1)}, u32[]{:S(2)}, u32[]{:S(2)}) collective-permute-start(bf16[272,256]{1,0:T(8,128)(2,1)} %get-tuple-element.22), channel_id=1, source_target_pairs={{0,32},{32,64},{64,96},{96,128},{128,160},{160,192},{192,224},{224... | collective-permute-start | bytes 417800 | tf_op jit(solution)/shard_map/ppermute | solution.py:245
  125.5 1.2 copy-start.3
  127.4 4.3 %copy-start.2 = (s32[4]{0:T(128)S(1)}, s32[4]{0:T(128)}, u32[]{:S(2)}) copy-start(s32[4]{0:T(128)} %pad_add_fusion.ids) | copy-start | bytes 52
  (1 other events, 0.7 us)
where the time goes:
time: 182 us; the launch traced here: 181 us
  blocking collectives  73.4 us (40%)
  starting transfers between devices  56.6 us (31%)
  waiting for transfers between devices  19.2 us (11%)
  Pallas kernels  18 us (10%)
  local copies, waits for them, and re-layouts  11 us (6%)
  other arithmetic  2.06 us (1%)
    all_to_all x1, blocking collectives, body(): lax.all_to_all(partial.reshape(n_tp, share, width), 'tp', 0, 0, tiled=True)  19 us
    ppermute x4, starting transfers between devices, body(): near.append(lax.ppermute(part, Z, [(n, (n + by) % 16) for n in range(16)]))  18.7 us
    all_to_all x1, blocking collectives, to_all(): lax.all_to_all(jnp.broadcast_to(x[None], (length, *x.shape)), axis, 0, 0,...  18.5 us
    pallas_call x7, Pallas kernels, call(): pl.pallas_call(kernel, out_shape=shapes[0] if one else shapes, in_specs=[...  18 us
    all_to_all x1, blocking collectives, body(): return lax.all_to_all(mixed, 'tp', 0, 0, tiled=True).reshape(rows, width)  16 us
    all_to_all x1, starting transfers between devices, to_all(): lax.all_to_all(jnp.broadcast_to(x[None], (length, *x.shape)), axis, 0, 0,...  12.4 us
    all_to_all x1, blocking collectives, body(): mine = lax.all_to_all(packed, plane, 0, 0, tiled=True)  10.1 us
    all_to_all x1, blocking collectives, body(): att = lax.all_to_all(att, plane, 0, 0, tiled=True)  9.91 us
  transfers between devices with their start and end apart: 14, of which 4 were waited for; matrix products, arithmetic and copies ran while one was open for 2% of the time, Pallas kernels for 7%

commit v1 on v0

--- a/solution.py
+++ b/solution.py
@@ -49,7 +49,7 @@
         out[i] = total
 
 
-def qkv_kernel(ids, b0, s0, b1, s1, b2, s2, b3, s3, w_in, qkv, docs, tail):
+def qkv_kernel(ids, b0, s0, b1, s1, b2, s2, b3, s3, w_in, qkv, docs, tail, head):
     rows = qkv.shape[0] // 8
     core, x = ids[0], ids[1]
     for back, pair in enumerate(((b0, s0), (b1, s1), (b2, s2), (b3, s3))):
@@ -58,6 +58,7 @@
             total = jnp.dot(part[:rows, :], w_in[...], preferred_element_type=jnp.float32)
             qkv[pl.ds(pl.multiple_of(at * rows, rows), rows), :] = total.astype(jnp.bfloat16)
             docs[pl.ds(at, 1), :] = part[rows : rows + 16, :rows].astype(jnp.float32)[0:1]
+    head[...] = qkv[:rows, :]
     tail[:rows, :] = qkv[7 * rows :, :]
     tail[rows:, :] = jnp.broadcast_to(docs[7:8, :], (16, rows)).astype(jnp.bfloat16)
 
@@ -120,11 +121,11 @@
     attend(range(2), ids, qkv, halo, docs, line, out)
 
 
-def order_kernel(ids, own, below, above, low, high, w_all, rows_out):
+def order_kernel(ids, own, below, above, second, w_all, rows_out):
     lanes = own.shape[1]
-    for ahead, part, first in ((0, own, 0), (3, below, 0), (1, above, 0), (2, low, 0), (2, high, low.shape[0])):
+    for ahead, part in ((0, own), (3, below), (1, above), (2, second)):
         for i in range(part.shape[0]):
-            z = (first + i) * 4 + ((ids[2] + ahead) & 3)
+            z = i * 4 + ((ids[2] + ahead) & 3)
             w_all[pl.ds(pl.multiple_of(z * lanes, lanes), lanes), :] = part[i]
             rows_out[pl.ds(pl.multiple_of(z * 16, 16), 16), :] = jnp.concatenate(
                 [part[i, 16 * j : 16 * j + 16, 3 * HEAD_DIM :] for j in range(8)], axis=1
@@ -220,9 +221,8 @@
     over_far = to_all(mine, "zh")
     over_far, line, at = lax.optimization_barrier((over_far, line, at))
     near = []
-    two = over_far.shape[0] // 2
-    for by, part in ((1, over_far), (-1, over_far), (2, over_far[:two]), (-2, over_far[two:])):
-        near.append(lax.ppermute(part, Z, [(n, (n + by) % 16) for n in range(16)]))
+    for by in (1, -1, 2):
+        near.append(lax.ppermute(over_far, Z, [(n, (n + by) % 16) for n in range(16)]))
     w_in, rows_out = in_vmem(
         order_kernel,
         [
@@ -233,19 +233,20 @@
     )(ids, over_far, *near)
     w_mine = to_all(rows_out, "x")
     w_other = lax.ppermute(w_mine, "c", swap)
-    qkv, docs, tail = in_vmem(
+    qkv, docs, tail, head = in_vmem(
         qkv_kernel,
         [
             jax.ShapeDtypeStruct((group * rows, 4 * HEAD_DIM), bf),
             jax.ShapeDtypeStruct((group, rows), jnp.float32),
             jax.ShapeDtypeStruct((rows + 16, 4 * HEAD_DIM), bf),
-        ],
-        grant=None,
+            jax.ShapeDtypeStruct((rows, 4 * HEAD_DIM), bf),
+        ],
+        grant=24,
     )(ids, *parts, w_in)
     halo = lax.ppermute(tail, Z, [(i, i + 1) for i in range(15)])
     att_shape = jax.ShapeDtypeStruct((group, rows // 2, 2 * HEAD_DIM), bf)
     att = in_vmem(later_kernel, att_shape)(qkv, docs, line)
-    att = in_vmem(early_kernel, att_shape, flops=10**9)(ids, qkv, halo, docs, line, att)
+    att = in_vmem(early_kernel, att_shape, flops=10**9)(ids, head, halo, docs, line, att)
     att = lax.all_to_all(att, plane, 0, 0, tiled=True)
     partial = in_vmem(
         project_kernel,

time: 182 us -> 159 us (0.87)
  the two profiles are of different devices: /device:TPU:96 before, /device:TPU:32 now
where the time goes in v1:
time: 159 us
  blocking collectives  59 us (37%)
  starting transfers between devices  53.7 us (34%)
  waiting for transfers between devices  23.9 us (15%)
  Pallas kernels  14.7 us (9%)
  local copies, waits for them, and re-layouts  4.94 us (3%)
  other arithmetic  2.02 us (1%)
    all_to_all x1, blocking collectives, body(): lax.all_to_all(partial.reshape(n_tp, share, width), 'tp', 0, 0, tiled=True)  19 us
    all_to_all x1, waiting for transfers between devices, to_all(): lax.all_to_all(jnp.broadcast_to(x[None], (length, *x.shape)), axis, 0, 0,...  16.4 us
    all_to_all x1, blocking collectives, body(): return lax.all_to_all(mixed, 'tp', 0, 0, tiled=True).reshape(rows, width)  16 us
    pallas_call x7, Pallas kernels, call(): pl.pallas_call(kernel, out_shape=shapes[0] if one else shapes, in_specs=[...  14.7 us
    all_to_all x1, starting transfers between devices, to_all(): lax.all_to_all(jnp.broadcast_to(x[None], (length, *x.shape)), axis, 0, 0,...  14.2 us
    all_to_all x1, blocking collectives, to_all(): lax.all_to_all(jnp.broadcast_to(x[None], (length, *x.shape)), axis, 0, 0,...  14.1 us
    ppermute x3, starting transfers between devices, body(): got = lax.ppermute(block, 'x', [(i, (i + back) % 4) for i in range(4)])  11.9 us
    all_to_all x1, blocking collectives, body(): att = lax.all_to_all(att, plane, 0, 0, tiled=True)  9.91 us
  transfers between devices with their start and end apart: 14, of which 5 were waited for; matrix products, arithmetic and copies ran while one was open for 3% of the time, Pallas kernels for 6%

profile of v1, /device:TPU:32, one launch (start us, length us, event | category | flops | bytes accessed | tf_op | source)
XLA Modules:
  0.0 158.6 jit_solution(12545728438104796998)
XLA Ops:
  0.6 2.8 %shard_map.82 = (bf16[8,16,192]{2,1,0:T(8,128)(2,1)}, bf16[8,16,64]{2,1,0:T(8,128)(2,1)}, bf16[272,2048]{1,0:T(8,128)(2,1)}) custom-call(s32[4]{0:T(128)} %pad_add_fusion.ids, bf16[16,512]{1,0:T(8,128)(2,1)} %bitcast.25, bf16[16,512]{1,0:T(8,128)(2,1)} %bitcast.26, bf16[16,512]{1,0:T(8,128)(2,1)} %bitcast.27, bf16[16,2048]{1,0:T(8,128)(2,1)} %bitcast.24, ...), custom_call_target="tpu_custom_call" | custom-call | flops 1000000000 | bytes 4194304 | tf_op jit(solution)/shard_map/pallas_call | solution.py:157
  3.3 4.4 %all-to-all-start = ((bf16[8,16,192]{2,1,0:T(8,128)(2,1)}), bf16[8,16,192]{2,1,0:T(8,128)(2,1)S(1)}, u32[]{:S(2)}, u32[]{:S(2)}) async-start(bf16[8,16,192]{2,1,0:T(8,128)(2,1)} %get-tuple-element.18), calls=%async_computation | async-start | bytes 131072 | tf_op jit(solution)/shard_map/all_to_all | solution.py:216
  7.8 3.9 %collective-permute-start.1 = (bf16[272,2048]{1,0:T(8,128)(2,1)}, bf16[272,2048]{1,0:T(8,128)(2,1)S(1)}, u32[]{:S(2)}, u32[]{:S(2)}) collective-permute-start(bf16[272,2048]{1,0:T(8,128)(2,1)} %get-tuple-element.17.b0), channel_id=1, source_target_pairs={{0,8},{8,16},{16,24},{24,0},{1,9},{9,17},{17,25},{25,1},{2,10},{10... | collective-permute-start | bytes 3342344 | tf_op jit(solution)/shard_map/ppermute | solution.py:219
  11.7 4.6 %collective-permute-start.3 = (bf16[272,2048]{1,0:T(8,128)(2,1)}, bf16[272,2048]{1,0:T(8,128)(2,1)}, u32[]{:S(2)}, u32[]{:S(2)}) collective-permute-start(bf16[272,2048]{1,0:T(8,128)(2,1)} %get-tuple-element.17.b0), channel_id=1, source_target_pairs={{0,16},{8,24},{16,0},{24,8},{1,17},{9,25},{17,1},{25,9},{2,18},{10... | collective-permute-start | bytes 3342344 | tf_op jit(solution)/shard_map/ppermute | solution.py:219
  16.3 3.4 %collective-permute-start.5 = (bf16[272,2048]{1,0:T(8,128)(2,1)}, bf16[272,2048]{1,0:T(8,128)(2,1)}, u32[]{:S(2)}, u32[]{:S(2)}) collective-permute-start(bf16[272,2048]{1,0:T(8,128)(2,1)} %get-tuple-element.17.b0), channel_id=1, source_target_pairs={{0,24},{8,0},{16,8},{24,16},{1,25},{9,1},{17,9},{25,17},{2,26},{10... | collective-permute-start | bytes 3342344 | tf_op jit(solution)/shard_map/ppermute | solution.py:219
  21.3 14.2 %all-to-all-start.1 = ((bf16[4,128,256]{2,1,0:T(8,128)(2,1)}), bf16[4,128,256]{2,1,0:T(8,128)(2,1)S(1)}, u32[]{:S(2)}, u32[]{:S(2)}) async-start(bf16[4,128,256]{2,1,0:T(8,128)(2,1)} %broadcast_in_dim.30), calls=%async_computation.1 | async-start | bytes 524288 | tf_op jit(solution)/shard_map/all_to_all | solution.py:24
  39.3 16.4 %all-to-all-done.1.own = bf16[4,128,256]{2,1,0:T(8,128)(2,1)S(1)} async-done(((bf16[4,128,256]{2,1,0:T(8,128)(2,1)}), bf16[4,128,256]{2,1,0:T(8,128)(2,1)S(1)}, u32[]{:S(2)}, u32[]{:S(2)}) %all-to-all-start.1) | async-done | bytes 262176 | tf_op jit(solution)/shard_map/all_to_all | solution.py:24
  55.7 3.0 %collective-permute-start.7 = (bf16[4,128,256]{2,1,0:T(8,128)(2,1)S(1)}, bf16[4,128,256]{2,1,0:T(8,128)(2,1)S(1)}, u32[]{:S(2)}, u32[]{:S(2)}) collective-permute-start(bf16[4,128,256]{2,1,0:T(8,128)(2,1)S(1)} %all-to-all-done.1.own), channel_id=1, source_target_pairs={{0,32},{32,64},{64,96},{96,128},{128,160},{160,192},{192,224},{224... | collective-permute-start | bytes 786440 | tf_op jit(solution)/shard_map/ppermute | solution.py:225
  58.7 2.8 %collective-permute-start.8 = (bf16[4,128,256]{2,1,0:T(8,128)(2,1)S(1)}, bf16[4,128,256]{2,1,0:T(8,128)(2,1)S(1)}, u32[]{:S(2)}, u32[]{:S(2)}) collective-permute-start(bf16[4,128,256]{2,1,0:T(8,128)(2,1)S(1)} %all-to-all-done.1.own), channel_id=1, source_target_pairs={{0,480},{32,0},{64,32},{96,64},{128,96},{160,128},{192,160},{224,1... | collective-permute-start | bytes 786440 | tf_op jit(solution)/shard_map/ppermute | solution.py:225
  61.5 2.6 %collective-permute-done.7.below = bf16[4,128,256]{2,1,0:T(8,128)(2,1)S(1)} collective-permute-done((bf16[4,128,256]{2,1,0:T(8,128)(2,1)S(1)}, bf16[4,128,256]{2,1,0:T(8,128)(2,1)S(1)}, u32[]{:S(2)}, u32[]{:S(2)}) %collective-permute-start.7) | collective-permute-done | bytes 262176 | tf_op jit(solution)/shard_map/ppermute | solution.py:225
  64.1 2.7 %collective-permute-start.9 = (bf16[4,128,256]{2,1,0:T(8,128)(2,1)S(1)}, bf16[4,128,256]{2,1,0:T(8,128)(2,1)S(1)}, u32[]{:S(2)}, u32[]{:S(2)}) collective-permute-start(bf16[4,128,256]{2,1,0:T(8,128)(2,1)S(1)} %all-to-all-done.1.own), channel_id=1, source_target_pairs={{0,64},{32,96},{64,128},{96,160},{128,192},{160,224},{192,256},{22... | collective-permute-start | bytes 786440 | tf_op jit(solution)/shard_map/ppermute | solution.py:225
  67.0 1.9 %collective-permute-start = (bf16[272,2048]{1,0:T(8,128)(2,1)S(1)}, bf16[272,2048]{1,0:T(8,128)(2,1)S(1)}, u32[]{:S(2)}, u32[]{:S(2)}) collective-permute-start(bf16[272,2048]{1,0:T(8,128)(2,1)S(1)} %copy-done.2), channel_id=1, source_target_pairs={{0,4},{4,0},{1,5},{5,1},{2,6},{6,2},{3,7},{7,3},{8,12},{12,8},{9,1... | collective-permute-start | bytes 3342344 | tf_op jit(solution)/shard_map/ppermute | solution.py:215
  68.9 2.4 %collective-permute-start.2 = (bf16[272,2048]{1,0:T(8,128)(2,1)S(1)}, bf16[272,2048]{1,0:T(8,128)(2,1)S(1)}, u32[]{:S(2)}, u32[]{:S(2)}) collective-permute-start(bf16[272,2048]{1,0:T(8,128)(2,1)S(1)} %collective-permute-done.1.b1), channel_id=1, source_target_pairs={{0,4},{4,0},{1,5},{5,1},{2,6},{6,2},{3,7},{7,3},{8,12},{12,8},{9,1... | collective-permute-start | bytes 3342344 | tf_op jit(solution)/shard_map/ppermute | solution.py:220
  71.3 1.9 %collective-permute-start.4 = (bf16[272,2048]{1,0:T(8,128)(2,1)}, bf16[272,2048]{1,0:T(8,128)(2,1)S(1)}, u32[]{:S(2)}, u32[]{:S(2)}) collective-permute-start(bf16[272,2048]{1,0:T(8,128)(2,1)} %collective-permute-done.3.b2), channel_id=1, source_target_pairs={{0,4},{4,0},{1,5},{5,1},{2,6},{6,2},{3,7},{7,3},{8,12},{12,8},{9,1... | collective-permute-start | bytes 3342344 | tf_op jit(solution)/shard_map/ppermute | solution.py:220
  73.3 2.4 %collective-permute-start.6 = (bf16[272,2048]{1,0:T(8,128)(2,1)}, bf16[272,2048]{1,0:T(8,128)(2,1)S(1)}, u32[]{:S(2)}, u32[]{:S(2)}) collective-permute-start(bf16[272,2048]{1,0:T(8,128)(2,1)} %collective-permute-done.5.b3), channel_id=1, source_target_pairs={{0,4},{4,0},{1,5},{5,1},{2,6},{6,2},{3,7},{7,3},{8,12},{12,8},{9,1... | collective-permute-start | bytes 3342344 | tf_op jit(solution)/shard_map/ppermute | solution.py:220
  75.7 3.9 %collective-permute-done.9.second = bf16[4,128,256]{2,1,0:T(8,128)(2,1)S(1)} collective-permute-done((bf16[4,128,256]{2,1,0:T(8,128)(2,1)S(1)}, bf16[4,128,256]{2,1,0:T(8,128)(2,1)S(1)}, u32[]{:S(2)}, u32[]{:S(2)}) %collective-permute-start.9) | collective-permute-done | bytes 262176 | tf_op jit(solution)/shard_map/ppermute | solution.py:225
  80.3 14.1 %all_to_all.30.w_mine = bf16[4,256,512]{2,1,0:T(8,128)(2,1)S(1)} all-to-all(bf16[4,256,512]{2,1,0:T(8,128)(2,1)S(1)} %broadcast_in_dim.34), channel_id=1, replica_groups=mesh['zh'=4,'zl'=4,'x'=4,'c'=2,'tp'=4] {'x'}, dimensions={0} | all-to-all | bytes 2097152 | tf_op jit(solution)/shard_map/all_to_all | solution.py:24
  94.4 1.9 %collective-permute-start.11 = (bf16[4,256,512]{2,1,0:T(8,128)(2,1)S(1)}, bf16[4,256,512]{2,1,0:T(8,128)(2,1)S(1)}, u32[]{:S(2)}, u32[]{:S(2)}) collective-permute-start(bf16[4,256,512]{2,1,0:T(8,128)(2,1)S(1)} %all_to_all.30.w_mine), channel_id=1, source_target_pairs={{0,4},{4,0},{1,5},{5,1},{2,6},{6,2},{3,7},{7,3},{8,12},{12,8},{9,1... | collective-permute-start | bytes 3145736 | tf_op jit(solution)/shard_map/ppermute | solution.py:235
  96.4 4.0 %shard_map.84 = (bf16[2048,256]{1,0:T(8,128)(2,1)S(1)}, f32[8,256]{1,0:T(8,128)S(1)}, bf16[272,256]{1,0:T(8,128)(2,1)S(1)}, bf16[256,256]{1,0:T(8,128)(2,1)S(1)}) custom-call(s32[4]{0:T(128)S(1)} %copy-done.1, bf16[272,2048]{1,0:T(8,128)(2,1)S(1)} %copy-done.2, bf16[272,2048]{1,0:T(8,128)(2,1)S(1)} %collective-permute-done.s0, ...), custom_call_target="tpu_custom_call" | custom-call | flops 20000000000 | bytes 4194304 | tf_op jit(solution)/shard_map/pallas_call | solution.py:157
  100.4 4.2 %collective-permute-start.10 = (bf16[272,256]{1,0:T(8,128)(2,1)S(1)}, bf16[272,256]{1,0:T(8,128)(2,1)S(1)}, u32[]{:S(2)}, u32[]{:S(2)}) collective-permute-start(bf16[272,256]{1,0:T(8,128)(2,1)S(1)} %get-tuple-element.23), channel_id=1, source_target_pairs={{0,32},{32,64},{64,96},{96,128},{128,160},{160,192},{192,224},{224... | collective-permute-start | bytes 417800 | tf_op jit(solution)/shard_map/ppermute | solution.py:246
  104.6 4.2 %shard_map.85.later = bf16[8,128,128]{2,1,0:T(8,128)(2,1)S(1)} custom-call(bf16[2048,256]{1,0:T(8,128)(2,1)S(1)} %get-tuple-element.26.qkv, f32[8,256]{1,0:T(8,128)S(1)} %get-tuple-element.24.docs, f32[1,512]{1,0:T(1,128)S(1)} %maximum_maximum_fusion.line), custom_call_target="tpu_custom_call" | custom-call | flops 20000000000 | bytes 4194304 | tf_op jit(solution)/shard_map/pallas_call | solution.py:157
  111.0 9.9 %all_to_all.31.att = bf16[8,128,128]{2,1,0:T(8,128)(2,1)S(1)} all-to-all(bf16[8,128,128]{2,1,0:T(8,128)(2,1)S(1)} %shard_map.86), channel_id=1, replica_groups=mesh['zh'=4,'zl'=4,'x'=4,'c'=2,'tp'=4] {'x','c'}, dimensions={0} | all-to-all | bytes 524288 | tf_op jit(solution)/shard_map/all_to_all | solution.py:250
  122.4 19.0 %all_to_all.32.partial = bf16[4,64,2048]{2,1,0:T(8,128)(2,1)S(1)} all-to-all(bf16[4,64,2048]{2,1,0:T(8,128)(2,1)S(1)} %bitcast.19), channel_id=1, replica_groups=mesh['zh'=4,'zl'=4,'x'=4,'c'=2,'tp'=4] {'tp'}, dimensions={0} | all-to-all | bytes 2097152 | tf_op jit(solution)/shard_map/all_to_all | solution.py:256
  141.6 16.0 %all_to_all.33 = bf16[4,64,2048]{2,1,0:T(8,128)(2,1)S(1)} all-to-all(bf16[4,64,2048]{2,1,0:T(8,128)(2,1)S(1)} %shard_map.88), channel_id=1, replica_groups=mesh['zh'=4,'zl'=4,'x'=4,'c'=2,'tp'=4] {'tp'}, dimensions={0} | all-to-all | bytes 2097152 | tf_op jit(solution)/shard_map/all_to_all | solution.py:258
  (36 shorter events, 11.7 us)
Async XLA Ops:
  0.0 35.4 %copy-start = (f32[1,8,257]{2,1,0:T(8,128)S(1)}, f32[1,8,257]{2,1,0:T(8,128)}, u32[]{:S(2)}) copy-start(f32[1,8,257]{2,1,0:T(8,128)} %param.15) | copy-start | bytes 24676
  3.3 63.6 %copy-start.2 = (bf16[272,2048]{1,0:T(8,128)(2,1)S(1)}, bf16[272,2048]{1,0:T(8,128)(2,1)}, u32[]{:S(2)}) copy-start(bf16[272,2048]{1,0:T(8,128)(2,1)} %get-tuple-element.17.b0) | copy-start | bytes 3342340
  3.3 76.2 %copy-start.1 = (s32[4]{0:T(128)S(1)}, s32[4]{0:T(128)}, u32[]{:S(2)}) copy-start(s32[4]{0:T(128)} %pad_add_fusion.ids) | copy-start | bytes 52
  3.3 16.3 %all-to-all-start = ((bf16[8,16,192]{2,1,0:T(8,128)(2,1)}), bf16[8,16,192]{2,1,0:T(8,128)(2,1)S(1)}, u32[]{:S(2)}, u32[]{:S(2)}) async-start(bf16[8,16,192]{2,1,0:T(8,128)(2,1)} %get-tuple-element.18), calls=%async_computation | async-start | bytes 131072 | tf_op jit(solution)/shard_map/all_to_all | solution.py:216
  7.8 61.1 %collective-permute-start.1 = (bf16[272,2048]{1,0:T(8,128)(2,1)}, bf16[272,2048]{1,0:T(8,128)(2,1)S(1)}, u32[]{:S(2)}, u32[]{:S(2)}) collective-permute-start(bf16[272,2048]{1,0:T(8,128)(2,1)} %get-tuple-element.17.b0), channel_id=1, source_target_pairs={{0,8},{8,16},{16,24},{24,0},{1,9},{9,17},{17,25},{25,1},{2,10},{10... | collective-permute-start | bytes 3342344 | tf_op jit(solution)/shard_map/ppermute | solution.py:219
  11.7 59.6 %collective-permute-start.3 = (bf16[272,2048]{1,0:T(8,128)(2,1)}, bf16[272,2048]{1,0:T(8,128)(2,1)}, u32[]{:S(2)}, u32[]{:S(2)}) collective-permute-start(bf16[272,2048]{1,0:T(8,128)(2,1)} %get-tuple-element.17.b0), channel_id=1, source_target_pairs={{0,16},{8,24},{16,0},{24,8},{1,17},{9,25},{17,1},{25,9},{2,18},{10... | collective-permute-start | bytes 3342344 | tf_op jit(solution)/shard_map/ppermute | solution.py:219
  16.3 57.0 %collective-permute-start.5 = (bf16[272,2048]{1,0:T(8,128)(2,1)}, bf16[272,2048]{1,0:T(8,128)(2,1)}, u32[]{:S(2)}, u32[]{:S(2)}) collective-permute-start(bf16[272,2048]{1,0:T(8,128)(2,1)} %get-tuple-element.17.b0), channel_id=1, source_target_pairs={{0,24},{8,0},{16,8},{24,16},{1,25},{9,1},{17,9},{25,17},{2,26},{10... | collective-permute-start | bytes 3342344 | tf_op jit(solution)/shard_map/ppermute | solution.py:219
  21.3 34.4 %all-to-all-start.1 = ((bf16[4,128,256]{2,1,0:T(8,128)(2,1)}), bf16[4,128,256]{2,1,0:T(8,128)(2,1)S(1)}, u32[]{:S(2)}, u32[]{:S(2)}) async-start(bf16[4,128,256]{2,1,0:T(8,128)(2,1)} %broadcast_in_dim.30), calls=%async_computation.1 | async-start | bytes 524288 | tf_op jit(solution)/shard_map/all_to_all | solution.py:24
  55.7 8.4 %collective-permute-start.7 = (bf16[4,128,256]{2,1,0:T(8,128)(2,1)S(1)}, bf16[4,128,256]{2,1,0:T(8,128)(2,1)S(1)}, u32[]{:S(2)}, u32[]{:S(2)}) collective-permute-start(bf16[4,128,256]{2,1,0:T(8,128)(2,1)S(1)} %all-to-all-done.1.own), channel_id=1, source_target_pairs={{0,32},{32,64},{64,96},{96,128},{128,160},{160,192},{192,224},{224... | collective-permute-start | bytes 786440 | tf_op jit(solution)/shard_map/ppermute | solution.py:225
  58.7 8.3 %collective-permute-start.8 = (bf16[4,128,256]{2,1,0:T(8,128)(2,1)S(1)}, bf16[4,128,256]{2,1,0:T(8,128)(2,1)S(1)}, u32[]{:S(2)}, u32[]{:S(2)}) collective-permute-start(bf16[4,128,256]{2,1,0:T(8,128)(2,1)S(1)} %all-to-all-done.1.own), channel_id=1, source_target_pairs={{0,480},{32,0},{64,32},{96,64},{128,96},{160,128},{192,160},{224,1... | collective-permute-start | bytes 786440 | tf_op jit(solution)/shard_map/ppermute | solution.py:225
  64.1 15.4 %collective-permute-start.9 = (bf16[4,128,256]{2,1,0:T(8,128)(2,1)S(1)}, bf16[4,128,256]{2,1,0:T(8,128)(2,1)S(1)}, u32[]{:S(2)}, u32[]{:S(2)}) collective-permute-start(bf16[4,128,256]{2,1,0:T(8,128)(2,1)S(1)} %all-to-all-done.1.own), channel_id=1, source_target_pairs={{0,64},{32,96},{64,128},{96,160},{128,192},{160,224},{192,256},{22... | collective-permute-start | bytes 786440 | tf_op jit(solution)/shard_map/ppermute | solution.py:225
  67.0 29.4 %collective-permute-start = (bf16[272,2048]{1,0:T(8,128)(2,1)S(1)}, bf16[272,2048]{1,0:T(8,128)(2,1)S(1)}, u32[]{:S(2)}, u32[]{:S(2)}) collective-permute-start(bf16[272,2048]{1,0:T(8,128)(2,1)S(1)} %copy-done.2), channel_id=1, source_target_pairs={{0,4},{4,0},{1,5},{5,1},{2,6},{6,2},{3,7},{7,3},{8,12},{12,8},{9,1... | collective-permute-start | bytes 3342344 | tf_op jit(solution)/shard_map/ppermute | solution.py:215
  68.9 27.5 %collective-permute-start.2 = (bf16[272,2048]{1,0:T(8,128)(2,1)S(1)}, bf16[272,2048]{1,0:T(8,128)(2,1)S(1)}, u32[]{:S(2)}, u32[]{:S(2)}) collective-permute-start(bf16[272,2048]{1,0:T(8,128)(2,1)S(1)} %collective-permute-done.1.b1), channel_id=1, source_target_pairs={{0,4},{4,0},{1,5},{5,1},{2,6},{6,2},{3,7},{7,3},{8,12},{12,8},{9,1... | collective-permute-start | bytes 3342344 | tf_op jit(solution)/shard_map/ppermute | solution.py:220
  71.3 25.1 %collective-permute-start.4 = (bf16[272,2048]{1,0:T(8,128)(2,1)}, bf16[272,2048]{1,0:T(8,128)(2,1)S(1)}, u32[]{:S(2)}, u32[]{:S(2)}) collective-permute-start(bf16[272,2048]{1,0:T(8,128)(2,1)} %collective-permute-done.3.b2), channel_id=1, source_target_pairs={{0,4},{4,0},{1,5},{5,1},{2,6},{6,2},{3,7},{7,3},{8,12},{12,8},{9,1... | collective-permute-start | bytes 3342344 | tf_op jit(solution)/shard_map/ppermute | solution.py:220
  73.3 23.1 %collective-permute-start.6 = (bf16[272,2048]{1,0:T(8,128)(2,1)}, bf16[272,2048]{1,0:T(8,128)(2,1)S(1)}, u32[]{:S(2)}, u32[]{:S(2)}) collective-permute-start(bf16[272,2048]{1,0:T(8,128)(2,1)} %collective-permute-done.5.b3), channel_id=1, source_target_pairs={{0,4},{4,0},{1,5},{5,1},{2,6},{6,2},{3,7},{7,3},{8,12},{12,8},{9,1... | collective-permute-start | bytes 3342344 | tf_op jit(solution)/shard_map/ppermute | solution.py:220
  94.4 26.5 %collective-permute-start.11 = (bf16[4,256,512]{2,1,0:T(8,128)(2,1)S(1)}, bf16[4,256,512]{2,1,0:T(8,128)(2,1)S(1)}, u32[]{:S(2)}, u32[]{:S(2)}) collective-permute-start(bf16[4,256,512]{2,1,0:T(8,128)(2,1)S(1)} %all_to_all.30.w_mine), channel_id=1, source_target_pairs={{0,4},{4,0},{1,5},{5,1},{2,6},{6,2},{3,7},{7,3},{8,12},{12,8},{9,1... | collective-permute-start | bytes 3145736 | tf_op jit(solution)/shard_map/ppermute | solution.py:235
  100.4 9.3 %collective-permute-start.10 = (bf16[272,256]{1,0:T(8,128)(2,1)S(1)}, bf16[272,256]{1,0:T(8,128)(2,1)S(1)}, u32[]{:S(2)}, u32[]{:S(2)}) collective-permute-start(bf16[272,256]{1,0:T(8,128)(2,1)S(1)} %get-tuple-element.23), channel_id=1, source_target_pairs={{0,32},{32,64},{64,96},{96,128},{128,160},{160,192},{192,224},{224... | collective-permute-start | bytes 417800 | tf_op jit(solution)/shard_map/ppermute | solution.py:246

commit v2 on v1

--- a/solution.py
+++ b/solution.py
@@ -24,13 +24,12 @@
     return lax.all_to_all(jnp.broadcast_to(x[None], (length, *x.shape)), axis, 0, 0, tiled=True)
 
 
-def prep_kernel(ids, w_q, w_k, w_v, w_o, tokens, gain, docs, heads, rest, block):
+def prep_kernel(ids, w_q, w_k, w_v, w_o, tokens, gain, docs, heads, block):
     n = heads.shape[0]
     own = w_o[:, pl.ds(pl.multiple_of(ids[3] * n * HEAD_DIM, n * HEAD_DIM), n * HEAD_DIM)]
     for i in range(n):
         cols = slice(i * HEAD_DIM, (i + 1) * HEAD_DIM)
-        heads[i] = jnp.concatenate([w_q[:, cols], w_k[:, cols], w_v[:, cols]], axis=1)
-        rest[i] = own[:, cols]
+        heads[i] = jnp.concatenate([w_q[:, cols], w_k[:, cols], w_v[:, cols], own[:, cols]], axis=1)
     rows = tokens.shape[0]
     wide = tokens[...].astype(jnp.float32)
     scale = lax.rsqrt(jnp.mean(wide * wide, axis=1, keepdims=True) + EPS)
@@ -127,9 +126,8 @@
         for i in range(part.shape[0]):
             z = i * 4 + ((ids[2] + ahead) & 3)
             w_all[pl.ds(pl.multiple_of(z * lanes, lanes), lanes), :] = part[i]
-            rows_out[pl.ds(pl.multiple_of(z * 16, 16), 16), :] = jnp.concatenate(
-                [part[i, 16 * j : 16 * j + 16, 3 * HEAD_DIM :] for j in range(8)], axis=1
-            )
+    half = rows_out.shape[0]
+    rows_out[...] = jnp.concatenate([w_all[:half, 3 * HEAD_DIM :], w_all[half:, 3 * HEAD_DIM :]], axis=1)
 
 
 def project_kernel(ids, att, w_mine, w_other, out, lhs, rhs):
@@ -138,11 +136,13 @@
         lhs[:half, i * HEAD_DIM : (i + 1) * HEAD_DIM] = att[i, :, :HEAD_DIM]
         lhs[half:, i * HEAD_DIM : (i + 1) * HEAD_DIM] = att[i, :, HEAD_DIM:]
     core = ids[0]
-    for c, w in ((core, w_mine), (1 - core, w_other)):
-        for z in range(16):
-            for x in range(4):
-                to = pl.multiple_of(z * 128 + x * 32 + c * 16, 16)
-                rhs[pl.ds(to, 16), :] = w[x, z * 16 : z * 16 + 16, :]
+    cut = w_mine.shape[1]
+    for x in range(w_mine.shape[0]):
+        pair = [jnp.where(core == c, w_mine[x], w_other[x]) for c in range(2)]
+        cols = slice(2 * x * HEAD_DIM, 2 * (x + 1) * HEAD_DIM)
+        for k in range(2):
+            lanes = slice(k * HEAD_DIM, (k + 1) * HEAD_DIM)
+            rhs[k * cut : (k + 1) * cut, cols] = jnp.concatenate([p[:, lanes] for p in pair], axis=1)
     out[...] = lax.dot_general(
         lhs[...], rhs[...], (((1,), (1,)), ((), ())), preferred_element_type=jnp.float32
     ).astype(jnp.bfloat16)
@@ -197,11 +197,10 @@
     piece = w_query.shape[1]
     ids = jnp.stack([core, x, z, tp])
     sources = (w_query[0], w_key[0], w_value[0], w_out[0].T, tokens, norm_gain, documents[None, :])
-    packed, rest, block = in_vmem(
+    packed, block = in_vmem(
         prep_kernel,
         [
-            jax.ShapeDtypeStruct((group, piece, 3 * HEAD_DIM), bf),
-            jax.ShapeDtypeStruct((group, piece, HEAD_DIM), bf),
+            jax.ShapeDtypeStruct((group, piece, 4 * HEAD_DIM), bf),
             jax.ShapeDtypeStruct((rows + 16, width), bf),
         ],
         grant=None,
@@ -214,7 +213,7 @@
     swap = [(0, 1), (1, 0)]
     parts = [block, lax.ppermute(block, "c", swap)]
     mine = lax.all_to_all(packed, plane, 0, 0, tiled=True)
-    mine = jnp.concatenate([mine, rest], axis=2).reshape(group * piece, 4 * HEAD_DIM)
+    mine = mine.reshape(group * piece, 4 * HEAD_DIM)
     for back in (1, 2, 3):
         got = lax.ppermute(block, "x", [(i, (i + back) % 4) for i in range(4)])
         parts += [got, lax.ppermute(got, "c", swap)]
@@ -227,7 +226,7 @@
         order_kernel,
         [
             jax.ShapeDtypeStruct((width, 4 * HEAD_DIM), bf),
-            jax.ShapeDtypeStruct((16 * piece, local), bf),
+            jax.ShapeDtypeStruct((width // 2, 2 * HEAD_DIM), bf),
         ],
         flops=10**9,
     )(ids, over_far, *near)

time: 159 us -> 159 us (level)
  transfers between devices with their start and end apart: 14 -> 14, of which waited for: 5 -> 5; matrix products, arithmetic and copies ran while one was open for 3% -> 3% of each run, Pallas kernels for 6% -> 7%
where the time goes in v2:
time: 159 us; the launch traced here: 158 us
  blocking collectives  59 us (37%)
  starting transfers between devices  53.7 us (34%)
  waiting for transfers between devices  24 us (15%)
  Pallas kernels  15.1 us (9%)
  local copies, waits for them, and re-layouts  4.84 us (3%)
    all_to_all x1, blocking collectives, body(): lax.all_to_all(partial.reshape(n_tp, share, width), 'tp', 0, 0, tiled=True)  19 us
    all_to_all x1, waiting for transfers between devices, to_all(): lax.all_to_all(jnp.broadcast_to(x[None], (length, *x.shape)), axis, 0, 0,...  16.5 us
    all_to_all x1, blocking collectives, body(): return lax.all_to_all(mixed, 'tp', 0, 0, tiled=True).reshape(rows, width)  16 us
    pallas_call x7, Pallas kernels, call(): pl.pallas_call(kernel, out_shape=shapes[0] if one else shapes, in_specs=[...  15.1 us
    all_to_all x1, starting transfers between devices, to_all(): lax.all_to_all(jnp.broadcast_to(x[None], (length, *x.shape)), axis, 0, 0,...  14.2 us
    all_to_all x1, blocking collectives, to_all(): lax.all_to_all(jnp.broadcast_to(x[None], (length, *x.shape)), axis, 0, 0,...  14.1 us
    ppermute x3, starting transfers between devices, body(): got = lax.ppermute(block, 'x', [(i, (i + back) % 4) for i in range(4)])  11.9 us
    all_to_all x1, blocking collectives, body(): att = lax.all_to_all(att, plane, 0, 0, tiled=True)  9.91 us
  transfers between devices with their start and end apart: 14, of which 5 were waited for; matrix products, arithmetic and copies ran while one was open for 3% of the time, Pallas kernels for 7%

profile of v2, /device:TPU:32, one launch (start us, length us, event | category | flops | bytes accessed | tf_op | source)
XLA Modules:
  0.0 158.3 jit_solution(15873623835884396245)
XLA Ops:
  0.6 2.8 %shard_map.82 = (bf16[8,16,256]{2,1,0:T(8,128)(2,1)}, bf16[272,2048]{1,0:T(8,128)(2,1)}) custom-call(s32[4]{0:T(128)} %pad_add_fusion.ids, bf16[16,512]{1,0:T(8,128)(2,1)} %bitcast.25, bf16[16,512]{1,0:T(8,128)(2,1)} %bitcast.26, bf16[16,512]{1,0:T(8,128)(2,1)} %bitcast.27, bf16[16,2048]{1,0:T(8,128)(2,1)} %bitcast.24, bf16[256,2048]{1,0:T(8,128)(2,1)} %tokens.1, ...), custom_call_target="tpu_custom_call" | custom-call | flops 1000000000 | bytes 4194304 | tf_op jit(solution)/shard_map/pallas_call | solution.py:157
  3.4 4.4 %all-to-all-start = ((bf16[8,16,256]{2,1,0:T(8,128)(2,1)}), bf16[8,16,256]{2,1,0:T(8,128)(2,1)S(1)}, u32[]{:S(2)}, u32[]{:S(2)}) async-start(bf16[8,16,256]{2,1,0:T(8,128)(2,1)} %get-tuple-element.17), calls=%async_computation | async-start | bytes 131072 | tf_op jit(solution)/shard_map/all_to_all | solution.py:215
  7.8 3.9 %collective-permute-start.1 = (bf16[272,2048]{1,0:T(8,128)(2,1)}, bf16[272,2048]{1,0:T(8,128)(2,1)S(1)}, u32[]{:S(2)}, u32[]{:S(2)}) collective-permute-start(bf16[272,2048]{1,0:T(8,128)(2,1)} %get-tuple-element.16.b0), channel_id=1, source_target_pairs={{0,8},{8,16},{16,24},{24,0},{1,9},{9,17},{17,25},{25,1},{2,10},{10... | collective-permute-start | bytes 3342344 | tf_op jit(solution)/shard_map/ppermute | solution.py:218
  11.7 4.6 %collective-permute-start.3 = (bf16[272,2048]{1,0:T(8,128)(2,1)}, bf16[272,2048]{1,0:T(8,128)(2,1)}, u32[]{:S(2)}, u32[]{:S(2)}) collective-permute-start(bf16[272,2048]{1,0:T(8,128)(2,1)} %get-tuple-element.16.b0), channel_id=1, source_target_pairs={{0,16},{8,24},{16,0},{24,8},{1,17},{9,25},{17,1},{25,9},{2,18},{10... | collective-permute-start | bytes 3342344 | tf_op jit(solution)/shard_map/ppermute | solution.py:218
  16.3 3.4 %collective-permute-start.5 = (bf16[272,2048]{1,0:T(8,128)(2,1)}, bf16[272,2048]{1,0:T(8,128)(2,1)}, u32[]{:S(2)}, u32[]{:S(2)}) collective-permute-start(bf16[272,2048]{1,0:T(8,128)(2,1)} %get-tuple-element.16.b0), channel_id=1, source_target_pairs={{0,24},{8,0},{16,8},{24,16},{1,25},{9,1},{17,9},{25,17},{2,26},{10... | collective-permute-start | bytes 3342344 | tf_op jit(solution)/shard_map/ppermute | solution.py:218
  20.4 14.2 %all-to-all-start.1 = ((bf16[4,128,256]{2,1,0:T(8,128)(2,1)}), bf16[4,128,256]{2,1,0:T(8,128)(2,1)S(1)}, u32[]{:S(2)}, u32[]{:S(2)}) async-start(bf16[4,128,256]{2,1,0:T(8,128)(2,1)} %broadcast_in_dim.30), calls=%async_computation.1 | async-start | bytes 524288 | tf_op jit(solution)/shard_map/all_to_all | solution.py:24
  38.3 16.5 %all-to-all-done.1.own = bf16[4,128,256]{2,1,0:T(8,128)(2,1)S(1)} async-done(((bf16[4,128,256]{2,1,0:T(8,128)(2,1)}), bf16[4,128,256]{2,1,0:T(8,128)(2,1)S(1)}, u32[]{:S(2)}, u32[]{:S(2)}) %all-to-all-start.1) | async-done | bytes 262176 | tf_op jit(solution)/shard_map/all_to_all | solution.py:24
  54.9 3.0 %collective-permute-start.7 = (bf16[4,128,256]{2,1,0:T(8,128)(2,1)S(1)}, bf16[4,128,256]{2,1,0:T(8,128)(2,1)S(1)}, u32[]{:S(2)}, u32[]{:S(2)}) collective-permute-start(bf16[4,128,256]{2,1,0:T(8,128)(2,1)S(1)} %all-to-all-done.1.own), channel_id=1, source_target_pairs={{0,32},{32,64},{64,96},{96,128},{128,160},{160,192},{192,224},{224... | collective-permute-start | bytes 786440 | tf_op jit(solution)/shard_map/ppermute | solution.py:224
  57.9 2.8 %collective-permute-start.8 = (bf16[4,128,256]{2,1,0:T(8,128)(2,1)S(1)}, bf16[4,128,256]{2,1,0:T(8,128)(2,1)S(1)}, u32[]{:S(2)}, u32[]{:S(2)}) collective-permute-start(bf16[4,128,256]{2,1,0:T(8,128)(2,1)S(1)} %all-to-all-done.1.own), channel_id=1, source_target_pairs={{0,480},{32,0},{64,32},{96,64},{128,96},{160,128},{192,160},{224,1... | collective-permute-start | bytes 786440 | tf_op jit(solution)/shard_map/ppermute | solution.py:224
  60.7 2.6 %collective-permute-done.7.below = bf16[4,128,256]{2,1,0:T(8,128)(2,1)S(1)} collective-permute-done((bf16[4,128,256]{2,1,0:T(8,128)(2,1)S(1)}, bf16[4,128,256]{2,1,0:T(8,128)(2,1)S(1)}, u32[]{:S(2)}, u32[]{:S(2)}) %collective-permute-start.7) | collective-permute-done | bytes 262176 | tf_op jit(solution)/shard_map/ppermute | solution.py:224
  63.3 2.7 %collective-permute-start.9 = (bf16[4,128,256]{2,1,0:T(8,128)(2,1)S(1)}, bf16[4,128,256]{2,1,0:T(8,128)(2,1)S(1)}, u32[]{:S(2)}, u32[]{:S(2)}) collective-permute-start(bf16[4,128,256]{2,1,0:T(8,128)(2,1)S(1)} %all-to-all-done.1.own), channel_id=1, source_target_pairs={{0,64},{32,96},{64,128},{96,160},{128,192},{160,224},{192,256},{22... | collective-permute-start | bytes 786440 | tf_op jit(solution)/shard_map/ppermute | solution.py:224
  66.1 1.9 %collective-permute-start = (bf16[272,2048]{1,0:T(8,128)(2,1)S(1)}, bf16[272,2048]{1,0:T(8,128)(2,1)S(1)}, u32[]{:S(2)}, u32[]{:S(2)}) collective-permute-start(bf16[272,2048]{1,0:T(8,128)(2,1)S(1)} %copy-done.2), channel_id=1, source_target_pairs={{0,4},{4,0},{1,5},{5,1},{2,6},{6,2},{3,7},{7,3},{8,12},{12,8},{9,1... | collective-permute-start | bytes 3342344 | tf_op jit(solution)/shard_map/ppermute | solution.py:214
  68.1 2.4 %collective-permute-start.2 = (bf16[272,2048]{1,0:T(8,128)(2,1)S(1)}, bf16[272,2048]{1,0:T(8,128)(2,1)S(1)}, u32[]{:S(2)}, u32[]{:S(2)}) collective-permute-start(bf16[272,2048]{1,0:T(8,128)(2,1)S(1)} %collective-permute-done.1.b1), channel_id=1, source_target_pairs={{0,4},{4,0},{1,5},{5,1},{2,6},{6,2},{3,7},{7,3},{8,12},{12,8},{9,1... | collective-permute-start | bytes 3342344 | tf_op jit(solution)/shard_map/ppermute | solution.py:219
  70.5 1.9 %collective-permute-start.4 = (bf16[272,2048]{1,0:T(8,128)(2,1)}, bf16[272,2048]{1,0:T(8,128)(2,1)S(1)}, u32[]{:S(2)}, u32[]{:S(2)}) collective-permute-start(bf16[272,2048]{1,0:T(8,128)(2,1)} %collective-permute-done.3.b2), channel_id=1, source_target_pairs={{0,4},{4,0},{1,5},{5,1},{2,6},{6,2},{3,7},{7,3},{8,12},{12,8},{9,1... | collective-permute-start | bytes 3342344 | tf_op jit(solution)/shard_map/ppermute | solution.py:219
  72.4 2.4 %collective-permute-start.6 = (bf16[272,2048]{1,0:T(8,128)(2,1)}, bf16[272,2048]{1,0:T(8,128)(2,1)S(1)}, u32[]{:S(2)}, u32[]{:S(2)}) collective-permute-start(bf16[272,2048]{1,0:T(8,128)(2,1)} %collective-permute-done.5.b3), channel_id=1, source_target_pairs={{0,4},{4,0},{1,5},{5,1},{2,6},{6,2},{3,7},{7,3},{8,12},{12,8},{9,1... | collective-permute-start | bytes 3342344 | tf_op jit(solution)/shard_map/ppermute | solution.py:219
  74.9 3.9 %collective-permute-done.9.second = bf16[4,128,256]{2,1,0:T(8,128)(2,1)S(1)} collective-permute-done((bf16[4,128,256]{2,1,0:T(8,128)(2,1)S(1)}, bf16[4,128,256]{2,1,0:T(8,128)(2,1)S(1)}, u32[]{:S(2)}, u32[]{:S(2)}) %collective-permute-start.9) | collective-permute-done | bytes 262176 | tf_op jit(solution)/shard_map/ppermute | solution.py:224
  79.6 14.1 %all_to_all.30.w_mine = bf16[4,1024,128]{2,1,0:T(8,128)(2,1)S(1)} all-to-all(bf16[4,1024,128]{2,1,0:T(8,128)(2,1)S(1)} %broadcast_in_dim.34), channel_id=1, replica_groups=mesh['zh'=4,'zl'=4,'x'=4,'c'=2,'tp'=4] {'x'}, dimensions={0} | all-to-all | bytes 2097152 | tf_op jit(solution)/shard_map/all_to_all | solution.py:24
  93.7 1.9 %collective-permute-start.11 = (bf16[4,1024,128]{2,1,0:T(8,128)(2,1)S(1)}, bf16[4,1024,128]{2,1,0:T(8,128)(2,1)S(1)}, u32[]{:S(2)}, u32[]{:S(2)}) collective-permute-start(bf16[4,1024,128]{2,1,0:T(8,128)(2,1)S(1)} %all_to_all.30.w_mine), channel_id=1, source_target_pairs={{0,4},{4,0},{1,5},{5,1},{2,6},{6,2},{3,7},{7,3},{8,12},{12,8},{9,1... | collective-permute-start | bytes 3145736 | tf_op jit(solution)/shard_map/ppermute | solution.py:234
  95.7 4.0 %shard_map.84 = (bf16[2048,256]{1,0:T(8,128)(2,1)S(1)}, f32[8,256]{1,0:T(8,128)S(1)}, bf16[272,256]{1,0:T(8,128)(2,1)S(1)}, bf16[256,256]{1,0:T(8,128)(2,1)S(1)}) custom-call(s32[4]{0:T(128)S(1)} %copy-done.1, bf16[272,2048]{1,0:T(8,128)(2,1)S(1)} %copy-done.2, bf16[272,2048]{1,0:T(8,128)(2,1)S(1)} %collective-permute-done.s0, ...), custom_call_target="tpu_custom_call" | custom-call | flops 20000000000 | bytes 4194304 | tf_op jit(solution)/shard_map/pallas_call | solution.py:157
  99.7 4.2 %collective-permute-start.10 = (bf16[272,256]{1,0:T(8,128)(2,1)S(1)}, bf16[272,256]{1,0:T(8,128)(2,1)S(1)}, u32[]{:S(2)}, u32[]{:S(2)}) collective-permute-start(bf16[272,256]{1,0:T(8,128)(2,1)S(1)} %get-tuple-element.21), channel_id=1, source_target_pairs={{0,32},{32,64},{64,96},{96,128},{128,160},{160,192},{192,224},{224... | collective-permute-start | bytes 417800 | tf_op jit(solution)/shard_map/ppermute | solution.py:245
  103.9 4.2 %shard_map.85.later = bf16[8,128,128]{2,1,0:T(8,128)(2,1)S(1)} custom-call(bf16[2048,256]{1,0:T(8,128)(2,1)S(1)} %get-tuple-element.24.qkv, f32[8,256]{1,0:T(8,128)S(1)} %get-tuple-element.22.docs, f32[1,512]{1,0:T(1,128)S(1)} %maximum_maximum_fusion.line), custom_call_target="tpu_custom_call" | custom-call | flops 20000000000 | bytes 4194304 | tf_op jit(solution)/shard_map/pallas_call | solution.py:157
  110.3 9.9 %all_to_all.31.att = bf16[8,128,128]{2,1,0:T(8,128)(2,1)S(1)} all-to-all(bf16[8,128,128]{2,1,0:T(8,128)(2,1)S(1)} %shard_map.86), channel_id=1, replica_groups=mesh['zh'=4,'zl'=4,'x'=4,'c'=2,'tp'=4] {'x','c'}, dimensions={0} | all-to-all | bytes 524288 | tf_op jit(solution)/shard_map/all_to_all | solution.py:249
  122.1 19.0 %all_to_all.32.partial = bf16[4,64,2048]{2,1,0:T(8,128)(2,1)S(1)} all-to-all(bf16[4,64,2048]{2,1,0:T(8,128)(2,1)S(1)} %bitcast.19), channel_id=1, replica_groups=mesh['zh'=4,'zl'=4,'x'=4,'c'=2,'tp'=4] {'tp'}, dimensions={0} | all-to-all | bytes 2097152 | tf_op jit(solution)/shard_map/all_to_all | solution.py:255
  141.3 16.0 %all_to_all.33 = bf16[4,64,2048]{2,1,0:T(8,128)(2,1)S(1)} all-to-all(bf16[4,64,2048]{2,1,0:T(8,128)(2,1)S(1)} %shard_map.88), channel_id=1, replica_groups=mesh['zh'=4,'zl'=4,'x'=4,'c'=2,'tp'=4] {'tp'}, dimensions={0} | all-to-all | bytes 2097152 | tf_op jit(solution)/shard_map/all_to_all | solution.py:257
  (35 shorter events, 11.3 us)
Async XLA Ops:
  0.0 34.6 %copy-start = (f32[1,8,257]{2,1,0:T(8,128)S(1)}, f32[1,8,257]{2,1,0:T(8,128)}, u32[]{:S(2)}) copy-start(f32[1,8,257]{2,1,0:T(8,128)} %param.15) | copy-start | bytes 24676
  3.4 62.8 %copy-start.2 = (bf16[272,2048]{1,0:T(8,128)(2,1)S(1)}, bf16[272,2048]{1,0:T(8,128)(2,1)}, u32[]{:S(2)}) copy-start(bf16[272,2048]{1,0:T(8,128)(2,1)} %get-tuple-element.16.b0) | copy-start | bytes 3342340
  3.4 75.3 %copy-start.1 = (s32[4]{0:T(128)S(1)}, s32[4]{0:T(128)}, u32[]{:S(2)}) copy-start(s32[4]{0:T(128)} %pad_add_fusion.ids) | copy-start | bytes 52
  3.4 16.3 %all-to-all-start = ((bf16[8,16,256]{2,1,0:T(8,128)(2,1)}), bf16[8,16,256]{2,1,0:T(8,128)(2,1)S(1)}, u32[]{:S(2)}, u32[]{:S(2)}) async-start(bf16[8,16,256]{2,1,0:T(8,128)(2,1)} %get-tuple-element.17), calls=%async_computation | async-start | bytes 131072 | tf_op jit(solution)/shard_map/all_to_all | solution.py:215
  7.8 60.3 %collective-permute-start.1 = (bf16[272,2048]{1,0:T(8,128)(2,1)}, bf16[272,2048]{1,0:T(8,128)(2,1)S(1)}, u32[]{:S(2)}, u32[]{:S(2)}) collective-permute-start(bf16[272,2048]{1,0:T(8,128)(2,1)} %get-tuple-element.16.b0), channel_id=1, source_target_pairs={{0,8},{8,16},{16,24},{24,0},{1,9},{9,17},{17,25},{25,1},{2,10},{10... | collective-permute-start | bytes 3342344 | tf_op jit(solution)/shard_map/ppermute | solution.py:218
  11.7 58.8 %collective-permute-start.3 = (bf16[272,2048]{1,0:T(8,128)(2,1)}, bf16[272,2048]{1,0:T(8,128)(2,1)}, u32[]{:S(2)}, u32[]{:S(2)}) collective-permute-start(bf16[272,2048]{1,0:T(8,128)(2,1)} %get-tuple-element.16.b0), channel_id=1, source_target_pairs={{0,16},{8,24},{16,0},{24,8},{1,17},{9,25},{17,1},{25,9},{2,18},{10... | collective-permute-start | bytes 3342344 | tf_op jit(solution)/shard_map/ppermute | solution.py:218
  16.3 56.1 %collective-permute-start.5 = (bf16[272,2048]{1,0:T(8,128)(2,1)}, bf16[272,2048]{1,0:T(8,128)(2,1)}, u32[]{:S(2)}, u32[]{:S(2)}) collective-permute-start(bf16[272,2048]{1,0:T(8,128)(2,1)} %get-tuple-element.16.b0), channel_id=1, source_target_pairs={{0,24},{8,0},{16,8},{24,16},{1,25},{9,1},{17,9},{25,17},{2,26},{10... | collective-permute-start | bytes 3342344 | tf_op jit(solution)/shard_map/ppermute | solution.py:218
  20.4 34.4 %all-to-all-start.1 = ((bf16[4,128,256]{2,1,0:T(8,128)(2,1)}), bf16[4,128,256]{2,1,0:T(8,128)(2,1)S(1)}, u32[]{:S(2)}, u32[]{:S(2)}) async-start(bf16[4,128,256]{2,1,0:T(8,128)(2,1)} %broadcast_in_dim.30), calls=%async_computation.1 | async-start | bytes 524288 | tf_op jit(solution)/shard_map/all_to_all | solution.py:24
  54.9 8.4 %collective-permute-start.7 = (bf16[4,128,256]{2,1,0:T(8,128)(2,1)S(1)}, bf16[4,128,256]{2,1,0:T(8,128)(2,1)S(1)}, u32[]{:S(2)}, u32[]{:S(2)}) collective-permute-start(bf16[4,128,256]{2,1,0:T(8,128)(2,1)S(1)} %all-to-all-done.1.own), channel_id=1, source_target_pairs={{0,32},{32,64},{64,96},{96,128},{128,160},{160,192},{192,224},{224... | collective-permute-start | bytes 786440 | tf_op jit(solution)/shard_map/ppermute | solution.py:224
  57.9 8.3 %collective-permute-start.8 = (bf16[4,128,256]{2,1,0:T(8,128)(2,1)S(1)}, bf16[4,128,256]{2,1,0:T(8,128)(2,1)S(1)}, u32[]{:S(2)}, u32[]{:S(2)}) collective-permute-start(bf16[4,128,256]{2,1,0:T(8,128)(2,1)S(1)} %all-to-all-done.1.own), channel_id=1, source_target_pairs={{0,480},{32,0},{64,32},{96,64},{128,96},{160,128},{192,160},{224,1... | collective-permute-start | bytes 786440 | tf_op jit(solution)/shard_map/ppermute | solution.py:224
  63.3 15.4 %collective-permute-start.9 = (bf16[4,128,256]{2,1,0:T(8,128)(2,1)S(1)}, bf16[4,128,256]{2,1,0:T(8,128)(2,1)S(1)}, u32[]{:S(2)}, u32[]{:S(2)}) collective-permute-start(bf16[4,128,256]{2,1,0:T(8,128)(2,1)S(1)} %all-to-all-done.1.own), channel_id=1, source_target_pairs={{0,64},{32,96},{64,128},{96,160},{128,192},{160,224},{192,256},{22... | collective-permute-start | bytes 786440 | tf_op jit(solution)/shard_map/ppermute | solution.py:224
  66.1 29.5 %collective-permute-start = (bf16[272,2048]{1,0:T(8,128)(2,1)S(1)}, bf16[272,2048]{1,0:T(8,128)(2,1)S(1)}, u32[]{:S(2)}, u32[]{:S(2)}) collective-permute-start(bf16[272,2048]{1,0:T(8,128)(2,1)S(1)} %copy-done.2), channel_id=1, source_target_pairs={{0,4},{4,0},{1,5},{5,1},{2,6},{6,2},{3,7},{7,3},{8,12},{12,8},{9,1... | collective-permute-start | bytes 3342344 | tf_op jit(solution)/shard_map/ppermute | solution.py:214
  68.1 27.6 %collective-permute-start.2 = (bf16[272,2048]{1,0:T(8,128)(2,1)S(1)}, bf16[272,2048]{1,0:T(8,128)(2,1)S(1)}, u32[]{:S(2)}, u32[]{:S(2)}) collective-permute-start(bf16[272,2048]{1,0:T(8,128)(2,1)S(1)} %collective-permute-done.1.b1), channel_id=1, source_target_pairs={{0,4},{4,0},{1,5},{5,1},{2,6},{6,2},{3,7},{7,3},{8,12},{12,8},{9,1... | collective-permute-start | bytes 3342344 | tf_op jit(solution)/shard_map/ppermute | solution.py:219
  70.5 25.2 %collective-permute-start.4 = (bf16[272,2048]{1,0:T(8,128)(2,1)}, bf16[272,2048]{1,0:T(8,128)(2,1)S(1)}, u32[]{:S(2)}, u32[]{:S(2)}) collective-permute-start(bf16[272,2048]{1,0:T(8,128)(2,1)} %collective-permute-done.3.b2), channel_id=1, source_target_pairs={{0,4},{4,0},{1,5},{5,1},{2,6},{6,2},{3,7},{7,3},{8,12},{12,8},{9,1... | collective-permute-start | bytes 3342344 | tf_op jit(solution)/shard_map/ppermute | solution.py:219
  72.4 23.3 %collective-permute-start.6 = (bf16[272,2048]{1,0:T(8,128)(2,1)}, bf16[272,2048]{1,0:T(8,128)(2,1)S(1)}, u32[]{:S(2)}, u32[]{:S(2)}) collective-permute-start(bf16[272,2048]{1,0:T(8,128)(2,1)} %collective-permute-done.5.b3), channel_id=1, source_target_pairs={{0,4},{4,0},{1,5},{5,1},{2,6},{6,2},{3,7},{7,3},{8,12},{12,8},{9,1... | collective-permute-start | bytes 3342344 | tf_op jit(solution)/shard_map/ppermute | solution.py:219
  93.7 26.5 %collective-permute-start.11 = (bf16[4,1024,128]{2,1,0:T(8,128)(2,1)S(1)}, bf16[4,1024,128]{2,1,0:T(8,128)(2,1)S(1)}, u32[]{:S(2)}, u32[]{:S(2)}) collective-permute-start(bf16[4,1024,128]{2,1,0:T(8,128)(2,1)S(1)} %all_to_all.30.w_mine), channel_id=1, source_target_pairs={{0,4},{4,0},{1,5},{5,1},{2,6},{6,2},{3,7},{7,3},{8,12},{12,8},{9,1... | collective-permute-start | bytes 3145736 | tf_op jit(solution)/shard_map/ppermute | solution.py:234
  99.7 9.3 %collective-permute-start.10 = (bf16[272,256]{1,0:T(8,128)(2,1)S(1)}, bf16[272,256]{1,0:T(8,128)(2,1)S(1)}, u32[]{:S(2)}, u32[]{:S(2)}) collective-permute-start(bf16[272,256]{1,0:T(8,128)(2,1)S(1)} %get-tuple-element.21), channel_id=1, source_target_pairs={{0,32},{32,64},{64,96},{96,128},{128,160},{160,192},{192,224},{224... | collective-permute-start | bytes 417800 | tf_op jit(solution)/shard_map/ppermute | solution.py:245

commit v3 on v2

--- a/solution.py
+++ b/solution.py
@@ -8,6 +8,7 @@
 
 HEAD_DIM = 64
 SEG = 64
+GROUP = 14
 LEFT = 4
 REL_CLIP = 128
 EPS = 1e-06
@@ -88,26 +89,33 @@
             return qkv[(b - 2) * Q_BLOCK : (b + 1) * Q_BLOCK, cols]
         return jnp.concatenate([row_part(i, cols) for i in range(b - 2, b + 1)], axis=0)
 
-    for b in blocks:
-        across = jnp.broadcast_to(doc_part(b), (Q_BLOCK, Q_BLOCK)).T
-        same = jnp.concatenate([across == doc_part(i) for i in range(b - 2, b + 1)], axis=1)
-        scores = lax.dot_general(
-            qkv[b * Q_BLOCK : (b + 1) * Q_BLOCK, :HEAD_DIM],
-            key_rows(b, slice(HEAD_DIM, 2 * HEAD_DIM)),
-            (((1,), (1,)), ((), ())),
-            preferred_element_type=jnp.float32,
-        )
-        scores = jnp.where(same, scores * HEAD_DIM ** (-0.5) + bias, NEG)
-        peak = jnp.max(scores, axis=1, keepdims=True)
-        raised = jnp.exp(scores - peak)
-        total = jnp.sum(raised, axis=1, keepdims=True)
-        mixed = jnp.dot(
-            raised.astype(jnp.bfloat16),
-            key_rows(b, slice(2 * HEAD_DIM, 3 * HEAD_DIM)),
-            preferred_element_type=jnp.float32,
-        )
-        lane = b % 2 * HEAD_DIM
-        out[b // 2, :, lane : lane + HEAD_DIM] = (mixed / total).astype(jnp.bfloat16)
+    for first in range(0, len(blocks), GROUP):
+        group = blocks[first : first + GROUP]
+        scores = []
+        for b in group:
+            across = jnp.broadcast_to(doc_part(b), (Q_BLOCK, Q_BLOCK)).T
+            same = jnp.concatenate([across == doc_part(i) for i in range(b - 2, b + 1)], axis=1)
+            product = lax.dot_general(
+                qkv[b * Q_BLOCK : (b + 1) * Q_BLOCK, :HEAD_DIM],
+                key_rows(b, slice(HEAD_DIM, 2 * HEAD_DIM)),
+                (((1,), (1,)), ((), ())),
+                preferred_element_type=jnp.float32,
+            )
+            scores.append(jnp.where(same, product * HEAD_DIM ** (-0.5) + bias, NEG))
+        peaks = [jnp.max(s, axis=1, keepdims=True) for s in scores]
+        raised = [jnp.exp(s - p) for s, p in zip(scores, peaks)]
+        totals = [jnp.sum(r, axis=1, keepdims=True) for r in raised]
+        mixed = [
+            jnp.dot(
+                r.astype(jnp.bfloat16),
+                key_rows(b, slice(2 * HEAD_DIM, 3 * HEAD_DIM)),
+                preferred_element_type=jnp.float32,
+            )
+            for b, r in zip(group, raised)
+        ]
+        for b, m, t in zip(group, mixed, totals):
+            lane = b % 2 * HEAD_DIM
+            out[b // 2, :, lane : lane + HEAD_DIM] = (m / t).astype(jnp.bfloat16)
 
 
 def later_kernel(qkv, docs, line, out):

time: 159 us -> 159 us (level)
  Pallas kernels: 15.1 us -> 12.7 us
  waiting for transfers between devices: 24 us -> 26.2 us
    pallas_call x7, Pallas kernels: 15.1 us -> 12.7 us  [call(): pl.pallas_call(kernel, out_shape=shapes[0] if one else shapes, in_specs=[...]
    ppermute x1, waiting for transfers between devices: 0.82 us -> 3.01 us  [body(): halo = lax.ppermute(tail, Z, [(i, i + 1) for i in range(15)])]
  transfers between devices with their start and end apart: 14 -> 14, of which waited for: 5 -> 5; matrix products, arithmetic and copies ran while one was open for 3% -> 3% of each run, Pallas kernels for 7% -> 5%
where the time goes in v3:
time: 159 us; the launch traced here: 158 us
  blocking collectives  59 us (37%)
  starting transfers between devices  53.7 us (34%)
  waiting for transfers between devices  26.2 us (16%)
  Pallas kernels  12.7 us (8%)
  local copies, waits for them, and re-layouts  4.84 us (3%)
    all_to_all x1, blocking collectives, body(): lax.all_to_all(partial.reshape(n_tp, share, width), 'tp', 0, 0, tiled=True)  19 us
    all_to_all x1, waiting for transfers between devices, to_all(): lax.all_to_all(jnp.broadcast_to(x[None], (length, *x.shape)), axis, 0, 0,...  16.5 us
    all_to_all x1, blocking collectives, body(): return lax.all_to_all(mixed, 'tp', 0, 0, tiled=True).reshape(rows, width)  16 us
    all_to_all x1, starting transfers between devices, to_all(): lax.all_to_all(jnp.broadcast_to(x[None], (length, *x.shape)), axis, 0, 0,...  14.2 us
    all_to_all x1, blocking collectives, to_all(): lax.all_to_all(jnp.broadcast_to(x[None], (length, *x.shape)), axis, 0, 0,...  14.1 us
    pallas_call x7, Pallas kernels, call(): pl.pallas_call(kernel, out_shape=shapes[0] if one else shapes, in_specs=[...  12.7 us
    ppermute x3, starting transfers between devices, body(): got = lax.ppermute(block, 'x', [(i, (i + back) % 4) for i in range(4)])  11.9 us
    all_to_all x1, blocking collectives, body(): att = lax.all_to_all(att, plane, 0, 0, tiled=True)  9.91 us
  transfers between devices with their start and end apart: 14, of which 5 were waited for; matrix products, arithmetic and copies ran while one was open for 3% of the time, Pallas kernels for 5%

profile of v3, /device:TPU:32, one launch (start us, length us, event | category | flops | bytes accessed | tf_op | source)
XLA Modules:
  0.0 158.0 jit_solution(8178786711432001849)
XLA Ops:
  0.6 2.8 %shard_map.82 = (bf16[8,16,256]{2,1,0:T(8,128)(2,1)}, bf16[272,2048]{1,0:T(8,128)(2,1)}) custom-call(s32[4]{0:T(128)} %pad_add_fusion.ids, bf16[16,512]{1,0:T(8,128)(2,1)} %bitcast.25, bf16[16,512]{1,0:T(8,128)(2,1)} %bitcast.26, bf16[16,512]{1,0:T(8,128)(2,1)} %bitcast.27, bf16[16,2048]{1,0:T(8,128)(2,1)} %bitcast.24, bf16[256,2048]{1,0:T(8,128)(2,1)} %tokens.1, ...), custom_call_target="tpu_custom_call" | custom-call | flops 1000000000 | bytes 4194304 | tf_op jit(solution)/shard_map/pallas_call | solution.py:165
  3.4 4.4 %all-to-all-start = ((bf16[8,16,256]{2,1,0:T(8,128)(2,1)}), bf16[8,16,256]{2,1,0:T(8,128)(2,1)S(1)}, u32[]{:S(2)}, u32[]{:S(2)}) async-start(bf16[8,16,256]{2,1,0:T(8,128)(2,1)} %get-tuple-element.17), calls=%async_computation | async-start | bytes 131072 | tf_op jit(solution)/shard_map/all_to_all | solution.py:223
  7.8 3.9 %collective-permute-start.1 = (bf16[272,2048]{1,0:T(8,128)(2,1)}, bf16[272,2048]{1,0:T(8,128)(2,1)S(1)}, u32[]{:S(2)}, u32[]{:S(2)}) collective-permute-start(bf16[272,2048]{1,0:T(8,128)(2,1)} %get-tuple-element.16.b0), channel_id=1, source_target_pairs={{0,8},{8,16},{16,24},{24,0},{1,9},{9,17},{17,25},{25,1},{2,10},{10... | collective-permute-start | bytes 3342344 | tf_op jit(solution)/shard_map/ppermute | solution.py:226
  11.7 4.6 %collective-permute-start.3 = (bf16[272,2048]{1,0:T(8,128)(2,1)}, bf16[272,2048]{1,0:T(8,128)(2,1)}, u32[]{:S(2)}, u32[]{:S(2)}) collective-permute-start(bf16[272,2048]{1,0:T(8,128)(2,1)} %get-tuple-element.16.b0), channel_id=1, source_target_pairs={{0,16},{8,24},{16,0},{24,8},{1,17},{9,25},{17,1},{25,9},{2,18},{10... | collective-permute-start | bytes 3342344 | tf_op jit(solution)/shard_map/ppermute | solution.py:226
  16.3 3.4 %collective-permute-start.5 = (bf16[272,2048]{1,0:T(8,128)(2,1)}, bf16[272,2048]{1,0:T(8,128)(2,1)}, u32[]{:S(2)}, u32[]{:S(2)}) collective-permute-start(bf16[272,2048]{1,0:T(8,128)(2,1)} %get-tuple-element.16.b0), channel_id=1, source_target_pairs={{0,24},{8,0},{16,8},{24,16},{1,25},{9,1},{17,9},{25,17},{2,26},{10... | collective-permute-start | bytes 3342344 | tf_op jit(solution)/shard_map/ppermute | solution.py:226
  20.4 14.2 %all-to-all-start.1 = ((bf16[4,128,256]{2,1,0:T(8,128)(2,1)}), bf16[4,128,256]{2,1,0:T(8,128)(2,1)S(1)}, u32[]{:S(2)}, u32[]{:S(2)}) async-start(bf16[4,128,256]{2,1,0:T(8,128)(2,1)} %broadcast_in_dim.30), calls=%async_computation.1 | async-start | bytes 524288 | tf_op jit(solution)/shard_map/all_to_all | solution.py:25
  38.3 16.5 %all-to-all-done.1.own = bf16[4,128,256]{2,1,0:T(8,128)(2,1)S(1)} async-done(((bf16[4,128,256]{2,1,0:T(8,128)(2,1)}), bf16[4,128,256]{2,1,0:T(8,128)(2,1)S(1)}, u32[]{:S(2)}, u32[]{:S(2)}) %all-to-all-start.1) | async-done | bytes 262176 | tf_op jit(solution)/shard_map/all_to_all | solution.py:25
  54.9 3.0 %collective-permute-start.7 = (bf16[4,128,256]{2,1,0:T(8,128)(2,1)S(1)}, bf16[4,128,256]{2,1,0:T(8,128)(2,1)S(1)}, u32[]{:S(2)}, u32[]{:S(2)}) collective-permute-start(bf16[4,128,256]{2,1,0:T(8,128)(2,1)S(1)} %all-to-all-done.1.own), channel_id=1, source_target_pairs={{0,32},{32,64},{64,96},{96,128},{128,160},{160,192},{192,224},{224... | collective-permute-start | bytes 786440 | tf_op jit(solution)/shard_map/ppermute | solution.py:232
  57.9 2.8 %collective-permute-start.8 = (bf16[4,128,256]{2,1,0:T(8,128)(2,1)S(1)}, bf16[4,128,256]{2,1,0:T(8,128)(2,1)S(1)}, u32[]{:S(2)}, u32[]{:S(2)}) collective-permute-start(bf16[4,128,256]{2,1,0:T(8,128)(2,1)S(1)} %all-to-all-done.1.own), channel_id=1, source_target_pairs={{0,480},{32,0},{64,32},{96,64},{128,96},{160,128},{192,160},{224,1... | collective-permute-start | bytes 786440 | tf_op jit(solution)/shard_map/ppermute | solution.py:232
  60.7 2.6 %collective-permute-done.7.below = bf16[4,128,256]{2,1,0:T(8,128)(2,1)S(1)} collective-permute-done((bf16[4,128,256]{2,1,0:T(8,128)(2,1)S(1)}, bf16[4,128,256]{2,1,0:T(8,128)(2,1)S(1)}, u32[]{:S(2)}, u32[]{:S(2)}) %collective-permute-start.7) | collective-permute-done | bytes 262176 | tf_op jit(solution)/shard_map/ppermute | solution.py:232
  63.3 2.7 %collective-permute-start.9 = (bf16[4,128,256]{2,1,0:T(8,128)(2,1)S(1)}, bf16[4,128,256]{2,1,0:T(8,128)(2,1)S(1)}, u32[]{:S(2)}, u32[]{:S(2)}) collective-permute-start(bf16[4,128,256]{2,1,0:T(8,128)(2,1)S(1)} %all-to-all-done.1.own), channel_id=1, source_target_pairs={{0,64},{32,96},{64,128},{96,160},{128,192},{160,224},{192,256},{22... | collective-permute-start | bytes 786440 | tf_op jit(solution)/shard_map/ppermute | solution.py:232
  66.1 1.9 %collective-permute-start = (bf16[272,2048]{1,0:T(8,128)(2,1)S(1)}, bf16[272,2048]{1,0:T(8,128)(2,1)S(1)}, u32[]{:S(2)}, u32[]{:S(2)}) collective-permute-start(bf16[272,2048]{1,0:T(8,128)(2,1)S(1)} %copy-done.2), channel_id=1, source_target_pairs={{0,4},{4,0},{1,5},{5,1},{2,6},{6,2},{3,7},{7,3},{8,12},{12,8},{9,1... | collective-permute-start | bytes 3342344 | tf_op jit(solution)/shard_map/ppermute | solution.py:222
  68.1 2.4 %collective-permute-start.2 = (bf16[272,2048]{1,0:T(8,128)(2,1)S(1)}, bf16[272,2048]{1,0:T(8,128)(2,1)S(1)}, u32[]{:S(2)}, u32[]{:S(2)}) collective-permute-start(bf16[272,2048]{1,0:T(8,128)(2,1)S(1)} %collective-permute-done.1.b1), channel_id=1, source_target_pairs={{0,4},{4,0},{1,5},{5,1},{2,6},{6,2},{3,7},{7,3},{8,12},{12,8},{9,1... | collective-permute-start | bytes 3342344 | tf_op jit(solution)/shard_map/ppermute | solution.py:227
  70.5 1.9 %collective-permute-start.4 = (bf16[272,2048]{1,0:T(8,128)(2,1)}, bf16[272,2048]{1,0:T(8,128)(2,1)S(1)}, u32[]{:S(2)}, u32[]{:S(2)}) collective-permute-start(bf16[272,2048]{1,0:T(8,128)(2,1)} %collective-permute-done.3.b2), channel_id=1, source_target_pairs={{0,4},{4,0},{1,5},{5,1},{2,6},{6,2},{3,7},{7,3},{8,12},{12,8},{9,1... | collective-permute-start | bytes 3342344 | tf_op jit(solution)/shard_map/ppermute | solution.py:227
  72.4 2.4 %collective-permute-start.6 = (bf16[272,2048]{1,0:T(8,128)(2,1)}, bf16[272,2048]{1,0:T(8,128)(2,1)S(1)}, u32[]{:S(2)}, u32[]{:S(2)}) collective-permute-start(bf16[272,2048]{1,0:T(8,128)(2,1)} %collective-permute-done.5.b3), channel_id=1, source_target_pairs={{0,4},{4,0},{1,5},{5,1},{2,6},{6,2},{3,7},{7,3},{8,12},{12,8},{9,1... | collective-permute-start | bytes 3342344 | tf_op jit(solution)/shard_map/ppermute | solution.py:227
  74.9 3.9 %collective-permute-done.9.second = bf16[4,128,256]{2,1,0:T(8,128)(2,1)S(1)} collective-permute-done((bf16[4,128,256]{2,1,0:T(8,128)(2,1)S(1)}, bf16[4,128,256]{2,1,0:T(8,128)(2,1)S(1)}, u32[]{:S(2)}, u32[]{:S(2)}) %collective-permute-start.9) | collective-permute-done | bytes 262176 | tf_op jit(solution)/shard_map/ppermute | solution.py:232
  79.6 14.1 %all_to_all.30.w_mine = bf16[4,1024,128]{2,1,0:T(8,128)(2,1)S(1)} all-to-all(bf16[4,1024,128]{2,1,0:T(8,128)(2,1)S(1)} %broadcast_in_dim.34), channel_id=1, replica_groups=mesh['zh'=4,'zl'=4,'x'=4,'c'=2,'tp'=4] {'x'}, dimensions={0} | all-to-all | bytes 2097152 | tf_op jit(solution)/shard_map/all_to_all | solution.py:25
  95.7 4.0 %shard_map.84 = (bf16[2048,256]{1,0:T(8,128)(2,1)S(1)}, f32[8,256]{1,0:T(8,128)S(1)}, bf16[272,256]{1,0:T(8,128)(2,1)S(1)}, bf16[256,256]{1,0:T(8,128)(2,1)S(1)}) custom-call(s32[4]{0:T(128)S(1)} %copy-done.1, bf16[272,2048]{1,0:T(8,128)(2,1)S(1)} %copy-done.2, bf16[272,2048]{1,0:T(8,128)(2,1)S(1)} %collective-permute-done.s0, ...), custom_call_target="tpu_custom_call" | custom-call | flops 20000000000 | bytes 4194304 | tf_op jit(solution)/shard_map/pallas_call | solution.py:165
  99.7 4.2 %collective-permute-start.10 = (bf16[272,256]{1,0:T(8,128)(2,1)S(1)}, bf16[272,256]{1,0:T(8,128)(2,1)S(1)}, u32[]{:S(2)}, u32[]{:S(2)}) collective-permute-start(bf16[272,256]{1,0:T(8,128)(2,1)S(1)} %get-tuple-element.21), channel_id=1, source_target_pairs={{0,32},{32,64},{64,96},{96,128},{128,160},{160,192},{192,224},{224... | collective-permute-start | bytes 417800 | tf_op jit(solution)/shard_map/ppermute | solution.py:253
  103.9 2.1 %shard_map.85.later = bf16[8,128,128]{2,1,0:T(8,128)(2,1)S(1)} custom-call(bf16[2048,256]{1,0:T(8,128)(2,1)S(1)} %get-tuple-element.24.qkv, f32[8,256]{1,0:T(8,128)S(1)} %get-tuple-element.22.docs, f32[1,512]{1,0:T(1,128)S(1)} %maximum_maximum_fusion.line), custom_call_target="tpu_custom_call" | custom-call | flops 20000000000 | bytes 4194304 | tf_op jit(solution)/shard_map/pallas_call | solution.py:165
  105.9 3.0 %collective-permute-done.10.halo = bf16[272,256]{1,0:T(8,128)(2,1)S(1)} collective-permute-done((bf16[272,256]{1,0:T(8,128)(2,1)S(1)}, bf16[272,256]{1,0:T(8,128)(2,1)S(1)}, u32[]{:S(2)}, u32[]{:S(2)}) %collective-permute-start.10) | collective-permute-done | bytes 139296 | tf_op jit(solution)/shard_map/ppermute | solution.py:253
  110.1 9.9 %all_to_all.31.att = bf16[8,128,128]{2,1,0:T(8,128)(2,1)S(1)} all-to-all(bf16[8,128,128]{2,1,0:T(8,128)(2,1)S(1)} %shard_map.86), channel_id=1, replica_groups=mesh['zh'=4,'zl'=4,'x'=4,'c'=2,'tp'=4] {'x','c'}, dimensions={0} | all-to-all | bytes 524288 | tf_op jit(solution)/shard_map/all_to_all | solution.py:257
  121.9 19.0 %all_to_all.32.partial = bf16[4,64,2048]{2,1,0:T(8,128)(2,1)S(1)} all-to-all(bf16[4,64,2048]{2,1,0:T(8,128)(2,1)S(1)} %bitcast.19), channel_id=1, replica_groups=mesh['zh'=4,'zl'=4,'x'=4,'c'=2,'tp'=4] {'tp'}, dimensions={0} | all-to-all | bytes 2097152 | tf_op jit(solution)/shard_map/all_to_all | solution.py:263
  141.0 16.0 %all_to_all.33 = bf16[4,64,2048]{2,1,0:T(8,128)(2,1)S(1)} all-to-all(bf16[4,64,2048]{2,1,0:T(8,128)(2,1)S(1)} %shard_map.88), channel_id=1, replica_groups=mesh['zh'=4,'zl'=4,'x'=4,'c'=2,'tp'=4] {'tp'}, dimensions={0} | all-to-all | bytes 2097152 | tf_op jit(solution)/shard_map/all_to_all | solution.py:265
  (35 shorter events, 12.1 us)
Async XLA Ops:
  0.0 34.6 %copy-start = (f32[1,8,257]{2,1,0:T(8,128)S(1)}, f32[1,8,257]{2,1,0:T(8,128)}, u32[]{:S(2)}) copy-start(f32[1,8,257]{2,1,0:T(8,128)} %param.15) | copy-start | bytes 24676
  3.4 62.8 %copy-start.2 = (bf16[272,2048]{1,0:T(8,128)(2,1)S(1)}, bf16[272,2048]{1,0:T(8,128)(2,1)}, u32[]{:S(2)}) copy-start(bf16[272,2048]{1,0:T(8,128)(2,1)} %get-tuple-element.16.b0) | copy-start | bytes 3342340
  3.4 75.3 %copy-start.1 = (s32[4]{0:T(128)S(1)}, s32[4]{0:T(128)}, u32[]{:S(2)}) copy-start(s32[4]{0:T(128)} %pad_add_fusion.ids) | copy-start | bytes 52
  3.4 16.3 %all-to-all-start = ((bf16[8,16,256]{2,1,0:T(8,128)(2,1)}), bf16[8,16,256]{2,1,0:T(8,128)(2,1)S(1)}, u32[]{:S(2)}, u32[]{:S(2)}) async-start(bf16[8,16,256]{2,1,0:T(8,128)(2,1)} %get-tuple-element.17), calls=%async_computation | async-start | bytes 131072 | tf_op jit(solution)/shard_map/all_to_all | solution.py:223
  7.8 60.3 %collective-permute-start.1 = (bf16[272,2048]{1,0:T(8,128)(2,1)}, bf16[272,2048]{1,0:T(8,128)(2,1)S(1)}, u32[]{:S(2)}, u32[]{:S(2)}) collective-permute-start(bf16[272,2048]{1,0:T(8,128)(2,1)} %get-tuple-element.16.b0), channel_id=1, source_target_pairs={{0,8},{8,16},{16,24},{24,0},{1,9},{9,17},{17,25},{25,1},{2,10},{10... | collective-permute-start | bytes 3342344 | tf_op jit(solution)/shard_map/ppermute | solution.py:226
  11.7 58.8 %collective-permute-start.3 = (bf16[272,2048]{1,0:T(8,128)(2,1)}, bf16[272,2048]{1,0:T(8,128)(2,1)}, u32[]{:S(2)}, u32[]{:S(2)}) collective-permute-start(bf16[272,2048]{1,0:T(8,128)(2,1)} %get-tuple-element.16.b0), channel_id=1, source_target_pairs={{0,16},{8,24},{16,0},{24,8},{1,17},{9,25},{17,1},{25,9},{2,18},{10... | collective-permute-start | bytes 3342344 | tf_op jit(solution)/shard_map/ppermute | solution.py:226
  16.3 56.1 %collective-permute-start.5 = (bf16[272,2048]{1,0:T(8,128)(2,1)}, bf16[272,2048]{1,0:T(8,128)(2,1)}, u32[]{:S(2)}, u32[]{:S(2)}) collective-permute-start(bf16[272,2048]{1,0:T(8,128)(2,1)} %get-tuple-element.16.b0), channel_id=1, source_target_pairs={{0,24},{8,0},{16,8},{24,16},{1,25},{9,1},{17,9},{25,17},{2,26},{10... | collective-permute-start | bytes 3342344 | tf_op jit(solution)/shard_map/ppermute | solution.py:226
  20.4 34.4 %all-to-all-start.1 = ((bf16[4,128,256]{2,1,0:T(8,128)(2,1)}), bf16[4,128,256]{2,1,0:T(8,128)(2,1)S(1)}, u32[]{:S(2)}, u32[]{:S(2)}) async-start(bf16[4,128,256]{2,1,0:T(8,128)(2,1)} %broadcast_in_dim.30), calls=%async_computation.1 | async-start | bytes 524288 | tf_op jit(solution)/shard_map/all_to_all | solution.py:25
  54.9 8.4 %collective-permute-start.7 = (bf16[4,128,256]{2,1,0:T(8,128)(2,1)S(1)}, bf16[4,128,256]{2,1,0:T(8,128)(2,1)S(1)}, u32[]{:S(2)}, u32[]{:S(2)}) collective-permute-start(bf16[4,128,256]{2,1,0:T(8,128)(2,1)S(1)} %all-to-all-done.1.own), channel_id=1, source_target_pairs={{0,32},{32,64},{64,96},{96,128},{128,160},{160,192},{192,224},{224... | collective-permute-start | bytes 786440 | tf_op jit(solution)/shard_map/ppermute | solution.py:232
  57.9 8.3 %collective-permute-start.8 = (bf16[4,128,256]{2,1,0:T(8,128)(2,1)S(1)}, bf16[4,128,256]{2,1,0:T(8,128)(2,1)S(1)}, u32[]{:S(2)}, u32[]{:S(2)}) collective-permute-start(bf16[4,128,256]{2,1,0:T(8,128)(2,1)S(1)} %all-to-all-done.1.own), channel_id=1, source_target_pairs={{0,480},{32,0},{64,32},{96,64},{128,96},{160,128},{192,160},{224,1... | collective-permute-start | bytes 786440 | tf_op jit(solution)/shard_map/ppermute | solution.py:232
  63.3 15.4 %collective-permute-start.9 = (bf16[4,128,256]{2,1,0:T(8,128)(2,1)S(1)}, bf16[4,128,256]{2,1,0:T(8,128)(2,1)S(1)}, u32[]{:S(2)}, u32[]{:S(2)}) collective-permute-start(bf16[4,128,256]{2,1,0:T(8,128)(2,1)S(1)} %all-to-all-done.1.own), channel_id=1, source_target_pairs={{0,64},{32,96},{64,128},{96,160},{128,192},{160,224},{192,256},{22... | collective-permute-start | bytes 786440 | tf_op jit(solution)/shard_map/ppermute | solution.py:232
  66.1 29.5 %collective-permute-start = (bf16[272,2048]{1,0:T(8,128)(2,1)S(1)}, bf16[272,2048]{1,0:T(8,128)(2,1)S(1)}, u32[]{:S(2)}, u32[]{:S(2)}) collective-permute-start(bf16[272,2048]{1,0:T(8,128)(2,1)S(1)} %copy-done.2), channel_id=1, source_target_pairs={{0,4},{4,0},{1,5},{5,1},{2,6},{6,2},{3,7},{7,3},{8,12},{12,8},{9,1... | collective-permute-start | bytes 3342344 | tf_op jit(solution)/shard_map/ppermute | solution.py:222
  68.1 27.6 %collective-permute-start.2 = (bf16[272,2048]{1,0:T(8,128)(2,1)S(1)}, bf16[272,2048]{1,0:T(8,128)(2,1)S(1)}, u32[]{:S(2)}, u32[]{:S(2)}) collective-permute-start(bf16[272,2048]{1,0:T(8,128)(2,1)S(1)} %collective-permute-done.1.b1), channel_id=1, source_target_pairs={{0,4},{4,0},{1,5},{5,1},{2,6},{6,2},{3,7},{7,3},{8,12},{12,8},{9,1... | collective-permute-start | bytes 3342344 | tf_op jit(solution)/shard_map/ppermute | solution.py:227
  70.5 25.2 %collective-permute-start.4 = (bf16[272,2048]{1,0:T(8,128)(2,1)}, bf16[272,2048]{1,0:T(8,128)(2,1)S(1)}, u32[]{:S(2)}, u32[]{:S(2)}) collective-permute-start(bf16[272,2048]{1,0:T(8,128)(2,1)} %collective-permute-done.3.b2), channel_id=1, source_target_pairs={{0,4},{4,0},{1,5},{5,1},{2,6},{6,2},{3,7},{7,3},{8,12},{12,8},{9,1... | collective-permute-start | bytes 3342344 | tf_op jit(solution)/shard_map/ppermute | solution.py:227
  72.4 23.3 %collective-permute-start.6 = (bf16[272,2048]{1,0:T(8,128)(2,1)}, bf16[272,2048]{1,0:T(8,128)(2,1)S(1)}, u32[]{:S(2)}, u32[]{:S(2)}) collective-permute-start(bf16[272,2048]{1,0:T(8,128)(2,1)} %collective-permute-done.5.b3), channel_id=1, source_target_pairs={{0,4},{4,0},{1,5},{5,1},{2,6},{6,2},{3,7},{7,3},{8,12},{12,8},{9,1... | collective-permute-start | bytes 3342344 | tf_op jit(solution)/shard_map/ppermute | solution.py:227
  93.7 26.3 %collective-permute-start.11 = (bf16[4,1024,128]{2,1,0:T(8,128)(2,1)S(1)}, bf16[4,1024,128]{2,1,0:T(8,128)(2,1)S(1)}, u32[]{:S(2)}, u32[]{:S(2)}) collective-permute-start(bf16[4,1024,128]{2,1,0:T(8,128)(2,1)S(1)} %all_to_all.30.w_mine), channel_id=1, source_target_pairs={{0,4},{4,0},{1,5},{5,1},{2,6},{6,2},{3,7},{7,3},{8,12},{12,8},{9,1... | collective-permute-start | bytes 3145736 | tf_op jit(solution)/shard_map/ppermute | solution.py:242
  99.7 9.3 %collective-permute-start.10 = (bf16[272,256]{1,0:T(8,128)(2,1)S(1)}, bf16[272,256]{1,0:T(8,128)(2,1)S(1)}, u32[]{:S(2)}, u32[]{:S(2)}) collective-permute-start(bf16[272,256]{1,0:T(8,128)(2,1)S(1)} %get-tuple-element.21), channel_id=1, source_target_pairs={{0,32},{32,64},{64,96},{96,128},{128,160},{160,192},{192,224},{224... | collective-permute-start | bytes 417800 | tf_op jit(solution)/shard_map/ppermute | solution.py:253
